TPU v7x, 512 devices: a whole 4x4x16 slice. The times are simulated.
512 devices in a mesh: fs: 64 (over z, y), tp: 8 (over x, core).
Axes of the slice: x: 4, y: 4, z: 16, core: 2. Of those that a mesh axis runs over, the one named last changes fastest.
Arguments:
- tokens: bfloat16 [24576, 2048], P('fs'), may hold values from -6 to 6
- merged: bfloat16 [24576, 2048], P('fs'), may hold values from -6 to 6
- gain_first: float32 [2048], replicated, may hold values from 0.1 to 1.9
- gate_first: bfloat16 [2048, 2816], P('fs', 'tp'), may hold values from -0.125 to 0.125
- up_first: bfloat16 [2048, 2816], P('fs', 'tp'), may hold values from -0.125 to 0.125
- down_first: bfloat16 [2816, 2048], P('tp', 'fs'), may hold values from -0.21875 to 0.21875
- gain_second: float32 [2048], replicated, may hold values from 0.1 to 1.9
- gate_second: bfloat16 [2048, 2816], P('fs', 'tp'), may hold values from -0.125 to 0.125
- up_second: bfloat16 [2048, 2816], P('fs', 'tp'), may hold values from -0.125 to 0.125
- down_second: bfloat16 [2816, 2048], P('tp', 'fs'), may hold values from -0.21875 to 0.21875
Outputs:
- result: bfloat16 [24576, 2048], P('fs')
All inputs are finite; a program needn't handle non-finite values.
Results may differ from a plain program's by a relative error of at most 0.01.
Values may be sent and summed in bfloat16 or wider, within the bound.
No kernel may reach another device: no remote copies, remote signals or barrier semaphores. Data moves between devices by JAX's collectives and lax.ppermute only.
A program may use at most 64 MiB of HBM per device.

v0:
```python
import jax
import jax.numpy as jnp
from jax import lax
from jax.sharding import Mesh
from jax.sharding import PartitionSpec as P

FS = ("z", "y")
TP = ("x", "c")
EPS = 1e-06
NZ, NY, NX, NC = 16, 4, 4, 2

W_SCALE = 2.0**18
A_SCALE = 2.0**8


def norm_rows(values, gain):
    scale = lax.rsqrt(jnp.mean(values * values, axis=-1, keepdims=True) + EPS)
    return values * scale * gain


def swap_cores(x):
    return lax.ppermute(x, "c", [(0, 1), (1, 0)])


def side_by_side(mats, times=1):
    rows, columns = mats[0].shape
    return jnp.concatenate([jnp.pad(m, ((0, (times - 1) * rows), (0, -columns % 128))) for m in mats], axis=1)


def half_coded(w):
    return (w.astype(jnp.float32) * W_SCALE).astype(jnp.float16)


def plain(w):
    return (w.astype(jnp.float32) * (1.0 / W_SCALE)).astype(jnp.bfloat16)


def gather_weights(first, second):
    rows, width = first.shape
    second, first = lax.optimization_barrier((second, first))
    second_y = lax.all_gather(second, "y", axis=0, tiled=True)
    first_z = lax.all_gather(first, "z", axis=0, tiled=True)
    second_y, first_z = lax.optimization_barrier((second_y, first_z))
    block = second_y.reshape(NY, -1, width)[:, :rows].reshape(NY * rows, width)
    block, first_z = lax.optimization_barrier((block, first_z))
    second_whole = lax.all_gather(block, "z", axis=0, tiled=True)
    first_whole = lax.all_gather(first_z.reshape(NZ, rows, width), "y", axis=1, tiled=True)
    return first_whole.reshape(-1, width), second_whole


def thirds(whole):
    width = whole.shape[1] // 3
    return [whole[:, k * width : (k + 1) * width] for k in range(3)]


def folded(normed, gate_w, up_w):
    gate = jnp.dot(normed, gate_w, preferred_element_type=jnp.float32)
    up = jnp.dot(normed, up_w, preferred_element_type=jnp.float32)
    return (jax.nn.silu(gate) * up).astype(jnp.bfloat16)


def down_dot(hidden, down_t):
    return lax.dot_general(hidden, down_t, (((1,), (1,)), ((), ())), preferred_element_type=jnp.float32)


def pieces_at_owner(hidden, down_t, share):
    core = lax.axis_index("c")
    parts = hidden.reshape(NX, NC, share, hidden.shape[-1])
    other = lax.dynamic_index_in_dim(parts, 1 - core, 1, keepdims=False).reshape(NX * share, -1)
    mine = lax.dynamic_index_in_dim(parts, core, 1, keepdims=False).reshape(NX * share, -1)
    sent = swap_cores(down_dot(other, down_t).astype(jnp.bfloat16))
    chip = (down_dot(mine, down_t) + sent.astype(jnp.float32)).astype(jnp.bfloat16)
    return lax.all_to_all(chip.reshape(NX, share, -1), "x", 0, 0, tiled=True)


def added(pieces):
    return jnp.sum(pieces.astype(jnp.float32), axis=0)


def power_of_two(p):
    size = jnp.abs(p)
    out = jnp.ones(p.shape, jnp.float32)
    for bit in range(7):
        factor = jnp.where(p < 0, 2.0 ** -(2**bit), 2.0 ** (2**bit))
        out = jnp.where((size >> bit) & 1 == 1, out * factor, out)
    return out


def spread_rows(finished):
    share, width = finished.shape
    wide = finished.astype(jnp.float32)
    top = jnp.max(jnp.abs(wide), axis=1, keepdims=True)
    power = jnp.floor(jnp.log2(jnp.maximum(top, 2.0**-100)))
    power = jnp.clip(power, -100.0, 127.0)
    coded = wide * power_of_two(13 - power.astype(jnp.int32))
    tail = jnp.broadcast_to(power, (share, 128))
    sent = jnp.concatenate([coded, tail], axis=1).astype(jnp.float16)
    everyone = lax.all_gather(sent, TP, axis=0, tiled=True)
    back = power_of_two(everyone[:, width : width + 1].astype(jnp.float32).astype(jnp.int32) - 13)
    everyone, back = lax.optimization_barrier((everyone, back))
    return (everyone[:, :width].astype(jnp.float32) * back).astype(jnp.bfloat16)


def body(tokens, merged, gain_first, gate_first, up_first, down_first, gain_second, gate_second, up_second, down_second):
    rows = tokens.shape[0]
    share = rows // (NX * NC)
    core = lax.axis_index("c")
    offset = (lax.axis_index("x") * NC + core) * share
    offset, tokens = lax.optimization_barrier((offset, tokens))
    own_first = half_coded(side_by_side((gate_first, up_first, down_first.T)))
    own_second = side_by_side((gate_second, up_second, down_second.T), NY)
    first, second = (thirds(whole) for whole in gather_weights(own_first, own_second))
    first = [plain(w) for w in first]
    normed_first = norm_rows(tokens.astype(jnp.float32), gain_first).astype(jnp.bfloat16)
    hidden = folded(normed_first, first[0], first[1])
    pieces = pieces_at_owner(hidden, first[2], share)
    pieces, tokens, merged, gain_second, offset = lax.optimization_barrier((pieces, tokens, merged, gain_second, offset))
    first_sum = added(pieces)
    base = lax.dynamic_slice_in_dim(tokens, offset, share, 0).astype(jnp.float32)
    extra = lax.dynamic_slice_in_dim(merged, offset, share, 0).astype(jnp.float32)
    middle = base + extra + 0.5 * first_sum
    normed_share = norm_rows(middle, gain_second).astype(jnp.bfloat16)
    coded = (normed_share.astype(jnp.float32) * A_SCALE).astype(jnp.float16)
    everyone = lax.all_gather(coded, TP, axis=0, tiled=True)
    normed_second = (everyone.astype(jnp.float32) * (1.0 / A_SCALE)).astype(jnp.bfloat16)
    hidden_two = folded(normed_second, second[0], second[1])
    second_sum = added(pieces_at_owner(hidden_two, second[2], share))
    finished = (middle + 0.5 * second_sum).astype(jnp.bfloat16)
    return spread_rows(finished)


def solution(mesh):
    finer = Mesh(mesh.devices.reshape(NZ, NY, NX, NC), ("z", "y", "x", "c"))
    return jax.shard_map(
        body,
        mesh=finer,
        in_specs=(P(FS, None), P(FS, None), P(), P(FS, TP), P(FS, TP), P(TP, FS), P(), P(FS, TP), P(FS, TP), P(TP, FS)),
        out_specs=P(FS, None),
        check_vma=False,
    )
```

profile of v0, /device:TPU:1, one launch (start us, length us, event | category | flops | bytes accessed | tf_op | source)
XLA Modules:
  0.0 181.6 jit_solution(11179573505998231326)
XLA Ops:
  6.5 0.0 copy-start
  6.5 0.0 all-gather.7.cloned.1.call-start
  6.5 1.6 fusion.36
  8.2 0.8 multiply_convert_fusion.23
  9.0 0.0 all-gather.7.cloned.1.call-update
  9.0 0.0 all-gather.9.cloned.1.call-start
  9.0 37.7 %all-gather.10 = f16[512,1152]{1,0:T(8,128)(2,1)S(1)} all-gather(f16[32,1152]{1,0:T(8,128)(2,1)S(1)} %multiply_convert_fusion.23), channel_id=1, replica_groups=mesh['z'=16,'y'=4,'x'=4,'c'=2] {'z'}, dimensions={0}, use_global_device_ids=true | all-gather | bytes 1253376 | tf_op jit(solution)/shard_map/all_gather | solution.py:42
  46.7 0.0 all-gather.7.cloned.1.call-done
  46.7 1.7 slice.36
  48.4 0.0 all-gather.9.cloned.1.call-update
  48.4 0.0 copy-done
  48.4 0.4 fusion
  48.8 0.0 copy-start.3
  48.8 35.5 %all-gather.11 = f16[16,128,1152]{2,1,0:T(8,128)(2,1)S(1)} all-gather(f16[16,32,1152]{2,1,0:T(8,128)(2,1)S(1)} %bitcast.22), channel_id=1, replica_groups=mesh['z'=16,'y'=4,'x'=4,'c'=2] {'y'}, dimensions={1}, use_global_device_ids=true | all-gather | bytes 5898240 | tf_op jit(solution)/shard_map/all_gather | solution.py:47
  84.3 0.0 copy-done.3
  84.3 1.0 fusion.3
  85.4 1.1 fusion.22
  86.5 0.7 convolution_convert_fusion.1
  87.2 9.4 %collective-permute-start = (bf16[192,2048]{1,0:T(8,128)(2,1)S(1)}, bf16[192,2048]{1,0:T(8,128)(2,1)S(1)}, u32[]{:S(2)}, u32[]{:S(2)}) collective-permute-start(bf16[192,2048]{1,0:T(8,128)(2,1)S(1)} %convolution_convert_fusion.1), channel_id=1, source_target_pairs={{0,1},{1,0},{2,3},{3,2},{4,5},{5,4},{6,7},{7,6},{8,9},{9,8},{10,11... | collective-permute-start | bytes 2359304 | tf_op jit(solution)/shard_map/ppermute | solution.py:22
  96.7 1.9 %collective-permute-done = bf16[192,2048]{1,0:T(8,128)(2,1)S(1)} collective-permute-done((bf16[192,2048]{1,0:T(8,128)(2,1)S(1)}, bf16[192,2048]{1,0:T(8,128)(2,1)S(1)}, u32[]{:S(2)}, u32[]{:S(2)}) %collective-permute-start) | collective-permute-done | bytes 786464 | tf_op jit(solution)/shard_map/ppermute | solution.py:22
  98.6 0.8 add_convert_fusion.1
  99.3 15.3 %all_to_all.10 = bf16[4,48,2048]{2,1,0:T(8,128)(2,1)S(1)} all-to-all(bf16[4,48,2048]{2,1,0:T(8,128)(2,1)S(1)} %bitcast.25), channel_id=1, replica_groups=mesh['z'=16,'y'=4,'x'=4,'c'=2] {'x'}, dimensions={0} | all-to-all | bytes 1572864 | tf_op jit(solution)/shard_map/all_to_all | solution.py:73
  114.6 0.0 copy-start.2
  114.6 0.1 convert_reduce_fusion.1
  114.7 1.2 multiply_reduce_fusion
  115.9 0.0 copy-done.2
  116.0 0.1 multiply_convert_fusion.21
  116.1 16.3 %all-gather.12 = f16[384,2048]{1,0:T(8,128)(2,1)S(1)} all-gather(f16[48,2048]{1,0:T(8,128)(2,1)S(1)} %multiply_convert_fusion.21), channel_id=1, replica_groups=mesh['z'=16,'y'=4,'x'=4,'c'=2] {'x','c'}, dimensions={0}, use_global_device_ids=true | all-gather | bytes 1769472 | tf_op jit(solution)/shard_map/all_gather | solution.py:124
  132.4 0.0 all-gather.9.cloned.1.call-done
  132.4 0.0 copy-start.1
  132.4 2.5 %fusion.7 = f32[384,384]{1,0:T(8,128)S(1)} fusion(bf16[2048,1152]{1,0:T(8,128)(2,1)} %all-gather.9.cloned.1.call-done, f16[384,2048]{1,0:T(8,128)(2,1)S(1)} %all-gather.12), kind=kOutput, calls=%fused_computation.16 | convolution fusion | flops 606339072 | bytes 3735552 | tf_op jit(solution)/shard_map/dot_general | solution.py:57
  134.9 0.3 copy-done.1
  135.2 1.0 fusion.23
  136.2 0.7 convolution_convert_fusion
  137.0 2.1 %collective-permute-start.1 = (bf16[192,2048]{1,0:T(8,128)(2,1)S(1)}, bf16[192,2048]{1,0:T(8,128)(2,1)S(1)}, u32[]{:S(2)}, u32[]{:S(2)}) collective-permute-start(bf16[192,2048]{1,0:T(8,128)(2,1)S(1)} %convolution_convert_fusion), channel_id=1, source_target_pairs={{0,1},{1,0},{2,3},{3,2},{4,5},{5,4},{6,7},{7,6},{8,9},{9,8},{10,11... | collective-permute-start | bytes 2359304 | tf_op jit(solution)/shard_map/ppermute | solution.py:22
  139.0 2.1 %collective-permute-done.1 = bf16[192,2048]{1,0:T(8,128)(2,1)S(1)} collective-permute-done((bf16[192,2048]{1,0:T(8,128)(2,1)S(1)}, bf16[192,2048]{1,0:T(8,128)(2,1)S(1)}, u32[]{:S(2)}, u32[]{:S(2)}) %collective-permute-start.1) | collective-permute-done | bytes 786464 | tf_op jit(solution)/shard_map/ppermute | solution.py:22
  141.1 0.7 add_convert_fusion
  141.9 14.5 %all_to_all.11 = bf16[4,48,2048]{2,1,0:T(8,128)(2,1)S(1)} all-to-all(bf16[4,48,2048]{2,1,0:T(8,128)(2,1)S(1)} %bitcast.23), channel_id=1, replica_groups=mesh['z'=16,'y'=4,'x'=4,'c'=2] {'x'}, dimensions={0} | all-to-all | bytes 1572864 | tf_op jit(solution)/shard_map/all_to_all | solution.py:73
  156.4 0.1 convert_reduce_fusion
  156.5 0.2 fusion.33
  156.7 0.1 fusion.34
  156.8 0.1 broadcast_in_dim.119
  156.9 0.1 pad_maximum_fusion
  156.9 15.9 %all-gather.13 = f16[384,2176]{1,0:T(8,128)(2,1)S(1)} all-gather(f16[48,2176]{1,0:T(8,128)(2,1)S(1)} %pad_maximum_fusion), channel_id=1, replica_groups=mesh['z'=16,'y'=4,'x'=4,'c'=2] {'x','c'}, dimensions={0}, use_global_device_ids=true | all-gather | bytes 1880064 | tf_op jit(solution)/shard_map/all_gather | solution.py:98
  172.9 0.3 multiply_select_fusion
  173.2 0.1 reduce
  173.3 1.5 multiply_convert_fusion
  (5 shorter events, 0.1 us)
Async XLA Ops:
  6.5 41.9 %copy-start = (bf16[384,2048]{1,0:T(8,128)(2,1)S(1)}, bf16[384,2048]{1,0:T(8,128)(2,1)}, u32[]{:S(2)}) copy-start(bf16[384,2048]{1,0:T(8,128)(2,1)} %param.10) | copy-start | bytes 4718596
  6.5 40.2 %all-gather.7.cloned.1.call-start = ((), (), s32[]{:S(2)}) async-start(), calls=%async_computation.2 | async-start | bytes 1474560 | tf_op jit(solution)/shard_map/all_gather | solution.py:41
  9.0 123.4 %all-gather.9.cloned.1.call-start = ((), (), s32[]{:S(2)}) async-start(), calls=%async_computation.3 | async-start | bytes 5013504 | tf_op jit(solution)/shard_map/all_gather | solution.py:46
  48.8 35.5 %copy-start.3 = (f32[2048]{0:T(1024)S(1)}, f32[2048]{0:T(1024)}, u32[]{:S(2)}) copy-start(f32[2048]{0:T(1024)} %param.12) | copy-start | bytes 24580
  87.2 11.3 %collective-permute-start = (bf16[192,2048]{1,0:T(8,128)(2,1)S(1)}, bf16[192,2048]{1,0:T(8,128)(2,1)S(1)}, u32[]{:S(2)}, u32[]{:S(2)}) collective-permute-start(bf16[192,2048]{1,0:T(8,128)(2,1)S(1)} %convolution_convert_fusion.1), channel_id=1, source_target_pairs={{0,1},{1,0},{2,3},{3,2},{4,5},{5,4},{6,7},{7,6},{8,9},{9,8},{10,11... | collective-permute-start | bytes 2359304 | tf_op jit(solution)/shard_map/ppermute | solution.py:22
  114.6 1.3 copy-start.2
  132.4 2.8 %copy-start.1 = (bf16[2048,1152]{1,0:T(8,128)(2,1)S(1)}, bf16[2048,1152]{1,0:T(8,128)(2,1)}, u32[]{:S(2)}) copy-start(bf16[2048,1152]{1,0:T(8,128)(2,1)} %all-gather.9.cloned.1.call-done) | copy-start | bytes 14155780
  137.0 4.2 %collective-permute-start.1 = (bf16[192,2048]{1,0:T(8,128)(2,1)S(1)}, bf16[192,2048]{1,0:T(8,128)(2,1)S(1)}, u32[]{:S(2)}, u32[]{:S(2)}) collective-permute-start(bf16[192,2048]{1,0:T(8,128)(2,1)S(1)} %convolution_convert_fusion), channel_id=1, source_target_pairs={{0,1},{1,0},{2,3},{3,2},{4,5},{5,4},{6,7},{7,6},{8,9},{9,8},{10,11... | collective-permute-start | bytes 2359304 | tf_op jit(solution)/shard_map/ppermute | solution.py:22
Sparse Core Ops, SparseCore 0:
  9.4 35.3 all-gather.6
  48.5 72.4 all-gather.8
where the time goes:
time: 182 us
  blocking collectives  135 us (74%)
  between operations  13.6 us (7%)
  starting transfers between devices  11.5 us (6%)
  matrix products  8.54 us (5%)
  other arithmetic  6.7 us (4%)
  waiting for transfers between devices  4.02 us (2%)
  local copies, waits for them, and re-layouts  2.15 us (1%)
    all_gather x1, blocking collectives, gather_weights(): first_z = lax.all_gather(first, 'z', axis=0, tiled=True)  37.7 us
    all_gather x1, blocking collectives, gather_weights(): lax.all_gather(first_z.reshape(NZ, rows, width), 'y', axis=1, tiled=True)  35.5 us
    all_to_all x2, blocking collectives, pieces_at_owner(): return lax.all_to_all(chip.reshape(NX, share, -1), 'x', 0, 0, tiled=True)  29.8 us
    all_gather x1, blocking collectives, body(): everyone = lax.all_gather(coded, TP, axis=0, tiled=True)  16.3 us
    all_gather x1, blocking collectives, spread_rows(): everyone = lax.all_gather(sent, TP, axis=0, tiled=True)  15.9 us
    ppermute x2, starting transfers between devices, swap_cores(): return lax.ppermute(x, 'c', [(0, 1), (1, 0)])  11.5 us
    ppermute x2, waiting for transfers between devices, swap_cores(): return lax.ppermute(x, 'c', [(0, 1), (1, 0)])  3.98 us
  transfers between devices with their start and end apart: 4, of which 2 were waited for; matrix products, arithmetic and copies ran while one was open for 3% of the time, Pallas kernels for 0%

commit v1 on v0

--- a/solution.py
+++ b/solution.py
@@ -109,15 +109,19 @@
     offset, tokens = lax.optimization_barrier((offset, tokens))
     own_first = half_coded(side_by_side((gate_first, up_first, down_first.T)))
     own_second = side_by_side((gate_second, up_second, down_second.T), NY)
-    first, second = (thirds(whole) for whole in gather_weights(own_first, own_second))
+    first, second = gather_weights(own_first, own_second)
+    first, tokens = lax.optimization_barrier((first, tokens))
+    first, second = thirds(first), thirds(second)
     first = [plain(w) for w in first]
     normed_first = norm_rows(tokens.astype(jnp.float32), gain_first).astype(jnp.bfloat16)
     hidden = folded(normed_first, first[0], first[1])
+    extra = lax.dynamic_slice_in_dim(merged, offset, share, 0)
+    hidden, extra = lax.optimization_barrier((hidden, extra))
     pieces = pieces_at_owner(hidden, first[2], share)
-    pieces, tokens, merged, gain_second, offset = lax.optimization_barrier((pieces, tokens, merged, gain_second, offset))
+    pieces, tokens, extra, gain_second, offset = lax.optimization_barrier((pieces, tokens, extra, gain_second, offset))
     first_sum = added(pieces)
     base = lax.dynamic_slice_in_dim(tokens, offset, share, 0).astype(jnp.float32)
-    extra = lax.dynamic_slice_in_dim(merged, offset, share, 0).astype(jnp.float32)
+    extra = extra.astype(jnp.float32)
     middle = base + extra + 0.5 * first_sum
     normed_share = norm_rows(middle, gain_second).astype(jnp.bfloat16)
     coded = (normed_share.astype(jnp.float32) * A_SCALE).astype(jnp.float16)

time: 182 us -> 182 us (level)
  no operation moved by 1% of the time
where the time goes in v1:
time: 182 us
  blocking collectives  135 us (74%)
  between operations  13.6 us (7%)
  starting transfers between devices  11.5 us (6%)
  matrix products  8.5 us (5%)
  other arithmetic  6.67 us (4%)
  waiting for transfers between devices  4.03 us (2%)
  local copies, waits for them, and re-layouts  2.51 us (1%)
    all_gather x1, blocking collectives, gather_weights(): first_z = lax.all_gather(first, 'z', axis=0, tiled=True)  37.7 us
    all_gather x1, blocking collectives, gather_weights(): lax.all_gather(first_z.reshape(NZ, rows, width), 'y', axis=1, tiled=True)  35.5 us
    all_to_all x2, blocking collectives, pieces_at_owner(): return lax.all_to_all(chip.reshape(NX, share, -1), 'x', 0, 0, tiled=True)  29.8 us
    all_gather x1, blocking collectives, body(): everyone = lax.all_gather(coded, TP, axis=0, tiled=True)  16.3 us
    all_gather x1, blocking collectives, spread_rows(): everyone = lax.all_gather(sent, TP, axis=0, tiled=True)  15.9 us
    ppermute x2, starting transfers between devices, swap_cores(): return lax.ppermute(x, 'c', [(0, 1), (1, 0)])  11.5 us
    ppermute x2, waiting for transfers between devices, swap_cores(): return lax.ppermute(x, 'c', [(0, 1), (1, 0)])  3.99 us
  transfers between devices with their start and end apart: 4, of which 2 were waited for; matrix products, arithmetic and copies ran while one was open for 3% of the time, Pallas kernels for 0%

profile of v1, /device:TPU:1, one launch (start us, length us, event | category | flops | bytes accessed | tf_op | source)
XLA Modules:
  0.0 182.0 jit_solution(7953924685720031888)
XLA Ops:
  6.5 0.0 copy-start
  6.5 0.0 all-gather.7.cloned.1.call-start
  6.5 1.6 fusion.36
  8.2 0.8 multiply_convert_fusion.23
  9.0 0.0 all-gather.7.cloned.1.call-update
  9.0 0.0 all-gather.9.cloned.1.call-start
  9.0 37.7 %all-gather.10 = f16[512,1152]{1,0:T(8,128)(2,1)S(1)} all-gather(f16[32,1152]{1,0:T(8,128)(2,1)S(1)} %multiply_convert_fusion.23), channel_id=1, replica_groups=mesh['z'=16,'y'=4,'x'=4,'c'=2] {'z'}, dimensions={0}, use_global_device_ids=true | all-gather | bytes 1253376 | tf_op jit(solution)/shard_map/all_gather | solution.py:42
  46.7 0.0 all-gather.7.cloned.1.call-done
  46.7 1.7 slice.36
  48.4 0.0 all-gather.9.cloned.1.call-update
  48.4 0.0 copy-done
  48.4 0.1 constant_dynamic-slice_fusion.4
  48.5 0.0 copy-start.1
  48.5 35.5 %all-gather.11 = f16[16,128,1152]{2,1,0:T(8,128)(2,1)S(1)} all-gather(f16[16,32,1152]{2,1,0:T(8,128)(2,1)S(1)} %bitcast.22), channel_id=1, replica_groups=mesh['z'=16,'y'=4,'x'=4,'c'=2] {'y'}, dimensions={1}, use_global_device_ids=true | all-gather | bytes 5898240 | tf_op jit(solution)/shard_map/all_gather | solution.py:47
  84.0 0.0 copy-start.4
  84.0 0.0 copy-done.1
  84.0 0.4 fusion
  84.4 0.3 copy-done.4
  84.7 1.0 fusion.3
  85.7 1.1 fusion.22
  86.9 0.7 convolution_convert_fusion.1
  87.6 9.4 %collective-permute-start = (bf16[192,2048]{1,0:T(8,128)(2,1)S(1)}, bf16[192,2048]{1,0:T(8,128)(2,1)S(1)}, u32[]{:S(2)}, u32[]{:S(2)}) collective-permute-start(bf16[192,2048]{1,0:T(8,128)(2,1)S(1)} %convolution_convert_fusion.1), channel_id=1, source_target_pairs={{0,1},{1,0},{2,3},{3,2},{4,5},{5,4},{6,7},{7,6},{8,9},{9,8},{10,11... | collective-permute-start | bytes 2359304 | tf_op jit(solution)/shard_map/ppermute | solution.py:22
  97.0 1.9 %collective-permute-done = bf16[192,2048]{1,0:T(8,128)(2,1)S(1)} collective-permute-done((bf16[192,2048]{1,0:T(8,128)(2,1)S(1)}, bf16[192,2048]{1,0:T(8,128)(2,1)S(1)}, u32[]{:S(2)}, u32[]{:S(2)}) %collective-permute-start) | collective-permute-done | bytes 786464 | tf_op jit(solution)/shard_map/ppermute | solution.py:22
  98.9 0.8 add_convert_fusion.1
  99.7 15.3 %all_to_all.10 = bf16[4,48,2048]{2,1,0:T(8,128)(2,1)S(1)} all-to-all(bf16[4,48,2048]{2,1,0:T(8,128)(2,1)S(1)} %bitcast.25), channel_id=1, replica_groups=mesh['z'=16,'y'=4,'x'=4,'c'=2] {'x'}, dimensions={0} | all-to-all | bytes 1572864 | tf_op jit(solution)/shard_map/all_to_all | solution.py:73
  115.0 0.1 convert_reduce_fusion.1
  115.1 1.2 multiply_reduce_fusion
  116.3 0.0 copy-done.3
  116.3 0.1 multiply_convert_fusion.21
  116.5 16.3 %all-gather.12 = f16[384,2048]{1,0:T(8,128)(2,1)S(1)} all-gather(f16[48,2048]{1,0:T(8,128)(2,1)S(1)} %multiply_convert_fusion.21), channel_id=1, replica_groups=mesh['z'=16,'y'=4,'x'=4,'c'=2] {'x','c'}, dimensions={0}, use_global_device_ids=true | all-gather | bytes 1769472 | tf_op jit(solution)/shard_map/all_gather | solution.py:128
  132.8 0.0 all-gather.9.cloned.1.call-done
  132.8 2.5 %fusion.7 = f32[384,384]{1,0:T(8,128)S(1)} fusion(bf16[2048,1152]{1,0:T(8,128)(2,1)} %all-gather.9.cloned.1.call-done, f16[384,2048]{1,0:T(8,128)(2,1)S(1)} %all-gather.12), kind=kOutput, calls=%fused_computation.16 | convolution fusion | flops 606339072 | bytes 3735552 | tf_op jit(solution)/shard_map/dot_general | solution.py:57
  135.3 0.3 copy-done.2
  135.6 1.0 fusion.23
  136.6 0.7 convolution_convert_fusion
  137.3 2.1 %collective-permute-start.1 = (bf16[192,2048]{1,0:T(8,128)(2,1)S(1)}, bf16[192,2048]{1,0:T(8,128)(2,1)S(1)}, u32[]{:S(2)}, u32[]{:S(2)}) collective-permute-start(bf16[192,2048]{1,0:T(8,128)(2,1)S(1)} %convolution_convert_fusion), channel_id=1, source_target_pairs={{0,1},{1,0},{2,3},{3,2},{4,5},{5,4},{6,7},{7,6},{8,9},{9,8},{10,11... | collective-permute-start | bytes 2359304 | tf_op jit(solution)/shard_map/ppermute | solution.py:22
  139.4 2.1 %collective-permute-done.1 = bf16[192,2048]{1,0:T(8,128)(2,1)S(1)} collective-permute-done((bf16[192,2048]{1,0:T(8,128)(2,1)S(1)}, bf16[192,2048]{1,0:T(8,128)(2,1)S(1)}, u32[]{:S(2)}, u32[]{:S(2)}) %collective-permute-start.1) | collective-permute-done | bytes 786464 | tf_op jit(solution)/shard_map/ppermute | solution.py:22
  141.5 0.7 add_convert_fusion
  142.2 14.5 %all_to_all.11 = bf16[4,48,2048]{2,1,0:T(8,128)(2,1)S(1)} all-to-all(bf16[4,48,2048]{2,1,0:T(8,128)(2,1)S(1)} %bitcast.23), channel_id=1, replica_groups=mesh['z'=16,'y'=4,'x'=4,'c'=2] {'x'}, dimensions={0} | all-to-all | bytes 1572864 | tf_op jit(solution)/shard_map/all_to_all | solution.py:73
  156.7 0.1 convert_reduce_fusion
  156.9 0.2 fusion.33
  157.1 0.1 fusion.34
  157.2 0.1 broadcast_in_dim.119
  157.2 0.1 pad_maximum_fusion
  157.3 15.9 %all-gather.13 = f16[384,2176]{1,0:T(8,128)(2,1)S(1)} all-gather(f16[48,2176]{1,0:T(8,128)(2,1)S(1)} %pad_maximum_fusion), channel_id=1, replica_groups=mesh['z'=16,'y'=4,'x'=4,'c'=2] {'x','c'}, dimensions={0}, use_global_device_ids=true | all-gather | bytes 1880064 | tf_op jit(solution)/shard_map/all_gather | solution.py:98
  173.2 0.3 multiply_select_fusion
  173.5 0.1 reduce
  173.7 1.5 multiply_convert_fusion
  (7 shorter events, 0.1 us)
Async XLA Ops:
  6.5 41.9 %copy-start = (bf16[384,2048]{1,0:T(8,128)(2,1)S(1)}, bf16[384,2048]{1,0:T(8,128)(2,1)}, u32[]{:S(2)}) copy-start(bf16[384,2048]{1,0:T(8,128)(2,1)} %param.11) | copy-start | bytes 4718596
  6.5 40.2 %all-gather.7.cloned.1.call-start = ((), (), s32[]{:S(2)}) async-start(), calls=%async_computation.2 | async-start | bytes 1474560 | tf_op jit(solution)/shard_map/all_gather | solution.py:41
  9.0 123.8 %all-gather.9.cloned.1.call-start = ((), (), s32[]{:S(2)}) async-start(), calls=%async_computation.3 | async-start | bytes 5013504 | tf_op jit(solution)/shard_map/all_gather | solution.py:46
  48.5 35.5 %copy-start.1 = (bf16[384,2048]{1,0:T(8,128)(2,1)S(1)}, bf16[384,2048]{1,0:T(8,128)(2,1)}, u32[]{:S(2)}) copy-start(bf16[384,2048]{1,0:T(8,128)(2,1)} %param.10) | copy-start | bytes 4718596
  84.0 0.7 copy-start.4
  87.6 11.3 %collective-permute-start = (bf16[192,2048]{1,0:T(8,128)(2,1)S(1)}, bf16[192,2048]{1,0:T(8,128)(2,1)S(1)}, u32[]{:S(2)}, u32[]{:S(2)}) collective-permute-start(bf16[192,2048]{1,0:T(8,128)(2,1)S(1)} %convolution_convert_fusion.1), channel_id=1, source_target_pairs={{0,1},{1,0},{2,3},{3,2},{4,5},{5,4},{6,7},{7,6},{8,9},{9,8},{10,11... | collective-permute-start | bytes 2359304 | tf_op jit(solution)/shard_map/ppermute | solution.py:22
  115.0 1.3 copy-start.3
  132.8 2.8 %copy-start.2 = (bf16[2048,1152]{1,0:T(8,128)(2,1)S(1)}, bf16[2048,1152]{1,0:T(8,128)(2,1)}, u32[]{:S(2)}) copy-start(bf16[2048,1152]{1,0:T(8,128)(2,1)} %all-gather.9.cloned.1.call-done) | copy-start | bytes 14155780
  137.3 4.2 %collective-permute-start.1 = (bf16[192,2048]{1,0:T(8,128)(2,1)S(1)}, bf16[192,2048]{1,0:T(8,128)(2,1)S(1)}, u32[]{:S(2)}, u32[]{:S(2)}) collective-permute-start(bf16[192,2048]{1,0:T(8,128)(2,1)S(1)} %convolution_convert_fusion), channel_id=1, source_target_pairs={{0,1},{1,0},{2,3},{3,2},{4,5},{5,4},{6,7},{7,6},{8,9},{9,8},{10,11... | collective-permute-start | bytes 2359304 | tf_op jit(solution)/shard_map/ppermute | solution.py:22
Sparse Core Ops, SparseCore 0:
  9.4 35.3 all-gather.6
  48.5 72.5 all-gather.8

commit v2 on v0

--- a/solution.py
+++ b/solution.py
@@ -113,11 +113,15 @@
     first = [plain(w) for w in first]
     normed_first = norm_rows(tokens.astype(jnp.float32), gain_first).astype(jnp.bfloat16)
     hidden = folded(normed_first, first[0], first[1])
+    extra = lax.dynamic_slice_in_dim(merged, offset, share, 0)
+    hidden, extra, tokens = lax.optimization_barrier((hidden, extra, tokens))
+    base = lax.dynamic_slice_in_dim(tokens, offset, share, 0)
+    hidden, base = lax.optimization_barrier((hidden, base))
     pieces = pieces_at_owner(hidden, first[2], share)
-    pieces, tokens, merged, gain_second, offset = lax.optimization_barrier((pieces, tokens, merged, gain_second, offset))
+    pieces, base, extra, gain_second = lax.optimization_barrier((pieces, base, extra, gain_second))
     first_sum = added(pieces)
-    base = lax.dynamic_slice_in_dim(tokens, offset, share, 0).astype(jnp.float32)
-    extra = lax.dynamic_slice_in_dim(merged, offset, share, 0).astype(jnp.float32)
+    base = base.astype(jnp.float32)
+    extra = extra.astype(jnp.float32)
     middle = base + extra + 0.5 * first_sum
     normed_share = norm_rows(middle, gain_second).astype(jnp.bfloat16)
     coded = (normed_share.astype(jnp.float32) * A_SCALE).astype(jnp.float16)

time: 182 us -> 184 us (1.011)
  no operation moved by 1% of the time
where the time goes in v2:
time: 184 us
  blocking collectives  136 us (74%)
  between operations  13.6 us (7%)
  starting transfers between devices  11.5 us (6%)
  matrix products  8.98 us (5%)
  other arithmetic  7.16 us (4%)
  waiting for transfers between devices  4.03 us (2%)
  local copies, waits for them, and re-layouts  2.76 us (2%)
    all_gather x1, blocking collectives, gather_weights(): first_z = lax.all_gather(first, 'z', axis=0, tiled=True)  37.7 us
    all_gather x1, blocking collectives, gather_weights(): lax.all_gather(first_z.reshape(NZ, rows, width), 'y', axis=1, tiled=True)  35.5 us
    all_to_all x2, blocking collectives, pieces_at_owner(): return lax.all_to_all(chip.reshape(NX, share, -1), 'x', 0, 0, tiled=True)  29.8 us
    all_gather x1, blocking collectives, body(): everyone = lax.all_gather(coded, TP, axis=0, tiled=True)  17 us
    all_gather x1, blocking collectives, spread_rows(): everyone = lax.all_gather(sent, TP, axis=0, tiled=True)  15.9 us
    ppermute x2, starting transfers between devices, swap_cores(): return lax.ppermute(x, 'c', [(0, 1), (1, 0)])  11.5 us
    dot_general x2, matrix products, folded(): gate = jnp.dot(normed, gate_w, preferred_element_type=jnp.float32)  4.05 us
    ppermute x2, waiting for transfers between devices, swap_cores(): return lax.ppermute(x, 'c', [(0, 1), (1, 0)])  3.99 us
  transfers between devices with their start and end apart: 4, of which 2 were waited for; matrix products, arithmetic and copies ran while one was open for 3% of the time, Pallas kernels for 0%

profile of v2, /device:TPU:1, one launch (start us, length us, event | category | flops | bytes accessed | tf_op | source)
XLA Modules:
  0.0 184.0 jit_solution(7150271148440579584)
XLA Ops:
  6.5 0.0 copy-start
  6.5 0.0 all-gather.7.cloned.1.call-start
  6.5 1.6 fusion.36
  8.2 0.8 multiply_convert_fusion.23
  9.0 0.0 all-gather.7.cloned.1.call-update
  9.0 0.0 all-gather.9.cloned.1.call-start
  9.0 37.7 %all-gather.10 = f16[512,1152]{1,0:T(8,128)(2,1)S(1)} all-gather(f16[32,1152]{1,0:T(8,128)(2,1)S(1)} %multiply_convert_fusion.23), channel_id=1, replica_groups=mesh['z'=16,'y'=4,'x'=4,'c'=2] {'z'}, dimensions={0}, use_global_device_ids=true | all-gather | bytes 1253376 | tf_op jit(solution)/shard_map/all_gather | solution.py:42
  46.7 1.7 slice.36
  48.4 0.0 all-gather.9.cloned.1.call-update
  48.4 1.8 fusion
  50.2 0.0 copy-done
  50.2 0.1 constant_dynamic-slice_fusion.5
  50.3 0.0 copy-start.1
  50.3 0.0 copy-start.5
  50.3 35.5 %all-gather.11 = f16[16,128,1152]{2,1,0:T(8,128)(2,1)S(1)} all-gather(f16[16,32,1152]{2,1,0:T(8,128)(2,1)S(1)} %bitcast.22), channel_id=1, replica_groups=mesh['z'=16,'y'=4,'x'=4,'c'=2] {'y'}, dimensions={1}, use_global_device_ids=true | all-gather | bytes 5898240 | tf_op jit(solution)/shard_map/all_gather | solution.py:47
  85.8 0.0 copy-done.1
  85.8 0.0 copy-done.5
  85.8 1.0 fusion.3
  86.9 1.1 fusion.22
  88.0 0.1 constant_dynamic-slice_fusion.4
  88.1 0.7 convolution_convert_fusion.1
  88.8 9.4 %collective-permute-start = (bf16[192,2048]{1,0:T(8,128)(2,1)S(1)}, bf16[192,2048]{1,0:T(8,128)(2,1)S(1)}, u32[]{:S(2)}, u32[]{:S(2)}) collective-permute-start(bf16[192,2048]{1,0:T(8,128)(2,1)S(1)} %convolution_convert_fusion.1), channel_id=1, source_target_pairs={{0,1},{1,0},{2,3},{3,2},{4,5},{5,4},{6,7},{7,6},{8,9},{9,8},{10,11... | collective-permute-start | bytes 2359304 | tf_op jit(solution)/shard_map/ppermute | solution.py:22
  98.2 1.9 %collective-permute-done = bf16[192,2048]{1,0:T(8,128)(2,1)S(1)} collective-permute-done((bf16[192,2048]{1,0:T(8,128)(2,1)S(1)}, bf16[192,2048]{1,0:T(8,128)(2,1)S(1)}, u32[]{:S(2)}, u32[]{:S(2)}) %collective-permute-start) | collective-permute-done | bytes 786464 | tf_op jit(solution)/shard_map/ppermute | solution.py:22
  100.1 0.8 add_convert_fusion.1
  100.9 0.0 copy-start.4
  100.9 15.3 %all_to_all.10 = bf16[4,48,2048]{2,1,0:T(8,128)(2,1)S(1)} all-to-all(bf16[4,48,2048]{2,1,0:T(8,128)(2,1)S(1)} %bitcast.25), channel_id=1, replica_groups=mesh['z'=16,'y'=4,'x'=4,'c'=2] {'x'}, dimensions={0} | all-to-all | bytes 1572864 | tf_op jit(solution)/shard_map/all_to_all | solution.py:73
  116.2 0.1 convert_reduce_fusion.1
  116.3 0.2 multiply_reduce_fusion
  116.5 0.0 copy-done.4
  116.6 0.1 multiply_convert_fusion.21
  116.7 17.0 %all-gather.12 = f16[384,2048]{1,0:T(8,128)(2,1)} all-gather(f16[48,2048]{1,0:T(8,128)(2,1)S(1)} %multiply_convert_fusion.21), channel_id=1, replica_groups=mesh['z'=16,'y'=4,'x'=4,'c'=2] {'x','c'}, dimensions={0}, use_global_device_ids=true | all-gather | bytes 1769472 | tf_op jit(solution)/shard_map/all_gather | solution.py:128
  133.7 3.0 %fusion.7 = f32[384,384]{1,0:T(8,128)S(1)} fusion(bf16[2048,1152]{1,0:T(8,128)(2,1)} %all-gather.9.cloned.1.call-done, f16[384,2048]{1,0:T(8,128)(2,1)} %all-gather.12), kind=kOutput, calls=%fused_computation.16 | convolution fusion | flops 606339072 | bytes 3735552 | tf_op jit(solution)/shard_map/dot_general | solution.py:57
  136.8 0.8 copy-done.3
  137.5 1.0 fusion.23
  138.6 0.7 convolution_convert_fusion
  139.3 2.1 %collective-permute-start.1 = (bf16[192,2048]{1,0:T(8,128)(2,1)S(1)}, bf16[192,2048]{1,0:T(8,128)(2,1)S(1)}, u32[]{:S(2)}, u32[]{:S(2)}) collective-permute-start(bf16[192,2048]{1,0:T(8,128)(2,1)S(1)} %convolution_convert_fusion), channel_id=1, source_target_pairs={{0,1},{1,0},{2,3},{3,2},{4,5},{5,4},{6,7},{7,6},{8,9},{9,8},{10,11... | collective-permute-start | bytes 2359304 | tf_op jit(solution)/shard_map/ppermute | solution.py:22
  141.3 2.1 %collective-permute-done.1 = bf16[192,2048]{1,0:T(8,128)(2,1)S(1)} collective-permute-done((bf16[192,2048]{1,0:T(8,128)(2,1)S(1)}, bf16[192,2048]{1,0:T(8,128)(2,1)S(1)}, u32[]{:S(2)}, u32[]{:S(2)}) %collective-permute-start.1) | collective-permute-done | bytes 786464 | tf_op jit(solution)/shard_map/ppermute | solution.py:22
  143.4 0.7 add_convert_fusion
  144.2 14.5 %all_to_all.11 = bf16[4,48,2048]{2,1,0:T(8,128)(2,1)S(1)} all-to-all(bf16[4,48,2048]{2,1,0:T(8,128)(2,1)S(1)} %bitcast.23), channel_id=1, replica_groups=mesh['z'=16,'y'=4,'x'=4,'c'=2] {'x'}, dimensions={0} | all-to-all | bytes 1572864 | tf_op jit(solution)/shard_map/all_to_all | solution.py:73
  158.7 0.1 convert_reduce_fusion
  158.8 0.2 fusion.33
  159.0 0.1 fusion.34
  159.2 0.1 broadcast_in_dim.119
  159.2 0.1 pad_maximum_fusion
  159.3 15.9 %all-gather.13 = f16[384,2176]{1,0:T(8,128)(2,1)S(1)} all-gather(f16[48,2176]{1,0:T(8,128)(2,1)S(1)} %pad_maximum_fusion), channel_id=1, replica_groups=mesh['z'=16,'y'=4,'x'=4,'c'=2] {'x','c'}, dimensions={0}, use_global_device_ids=true | all-gather | bytes 1880064 | tf_op jit(solution)/shard_map/all_gather | solution.py:98
  175.2 0.3 multiply_select_fusion
  175.5 0.1 reduce
  175.7 1.5 multiply_convert_fusion
  (10 shorter events, 0.1 us)
Async XLA Ops:
  6.5 43.7 %copy-start = (bf16[384,2048]{1,0:T(8,128)(2,1)S(1)}, bf16[384,2048]{1,0:T(8,128)(2,1)}, u32[]{:S(2)}) copy-start(bf16[384,2048]{1,0:T(8,128)(2,1)} %param.11) | copy-start | bytes 4718596
  6.5 40.2 %all-gather.7.cloned.1.call-start = ((), (), s32[]{:S(2)}) async-start(), calls=%async_computation.2 | async-start | bytes 1474560 | tf_op jit(solution)/shard_map/all_gather | solution.py:41
  9.0 124.7 %all-gather.9.cloned.1.call-start = ((), (), s32[]{:S(2)}) async-start(), calls=%async_computation.3 | async-start | bytes 5013504 | tf_op jit(solution)/shard_map/all_gather | solution.py:46
  50.3 35.5 %copy-start.1 = (bf16[384,2048]{1,0:T(8,128)(2,1)S(1)}, bf16[384,2048]{1,0:T(8,128)(2,1)}, u32[]{:S(2)}) copy-start(bf16[384,2048]{1,0:T(8,128)(2,1)} %param.10) | copy-start | bytes 4718596
  50.3 35.5 %copy-start.5 = (f32[2048]{0:T(1024)S(1)}, f32[2048]{0:T(1024)}, u32[]{:S(2)}) copy-start(f32[2048]{0:T(1024)} %param.12) | copy-start | bytes 24580
  88.8 11.3 %collective-permute-start = (bf16[192,2048]{1,0:T(8,128)(2,1)S(1)}, bf16[192,2048]{1,0:T(8,128)(2,1)S(1)}, u32[]{:S(2)}, u32[]{:S(2)}) collective-permute-start(bf16[192,2048]{1,0:T(8,128)(2,1)S(1)} %convolution_convert_fusion.1), channel_id=1, source_target_pairs={{0,1},{1,0},{2,3},{3,2},{4,5},{5,4},{6,7},{7,6},{8,9},{9,8},{10,11... | collective-permute-start | bytes 2359304 | tf_op jit(solution)/shard_map/ppermute | solution.py:22
  100.9 15.7 %copy-start.4 = (f32[2048]{0:T(1024)S(1)}, f32[2048]{0:T(1024)}, u32[]{:S(2)}) copy-start(f32[2048]{0:T(1024)} %param.16) | copy-start | bytes 24580
  133.7 3.0 %copy-start.2 = (f16[384,2048]{1,0:T(8,128)(2,1)S(1)}, f16[384,2048]{1,0:T(8,128)(2,1)}, u32[]{:S(2)}) copy-start(f16[384,2048]{1,0:T(8,128)(2,1)} %all-gather.12) | copy-start | bytes 4718596
  133.7 3.8 %copy-start.3 = (bf16[2048,1152]{1,0:T(8,128)(2,1)S(1)}, bf16[2048,1152]{1,0:T(8,128)(2,1)}, u32[]{:S(2)}) copy-start(bf16[2048,1152]{1,0:T(8,128)(2,1)} %all-gather.9.cloned.1.call-done) | copy-start | bytes 14155780
  139.3 4.2 %collective-permute-start.1 = (bf16[192,2048]{1,0:T(8,128)(2,1)S(1)}, bf16[192,2048]{1,0:T(8,128)(2,1)S(1)}, u32[]{:S(2)}, u32[]{:S(2)}) collective-permute-start(bf16[192,2048]{1,0:T(8,128)(2,1)S(1)} %convolution_convert_fusion), channel_id=1, source_target_pairs={{0,1},{1,0},{2,3},{3,2},{4,5},{5,4},{6,7},{7,6},{8,9},{9,8},{10,11... | collective-permute-start | bytes 2359304 | tf_op jit(solution)/shard_map/ppermute | solution.py:22
Sparse Core Ops, SparseCore 0:
  9.4 35.3 all-gather.6
  48.5 72.5 all-gather.8

commit v3 on v2

--- a/solution.py
+++ b/solution.py
@@ -109,7 +109,9 @@
     offset, tokens = lax.optimization_barrier((offset, tokens))
     own_first = half_coded(side_by_side((gate_first, up_first, down_first.T)))
     own_second = side_by_side((gate_second, up_second, down_second.T), NY)
-    first, second = (thirds(whole) for whole in gather_weights(own_first, own_second))
+    first, second = gather_weights(own_first, own_second)
+    first, tokens = lax.optimization_barrier((first, tokens))
+    first, second = thirds(first), thirds(second)
     first = [plain(w) for w in first]
     normed_first = norm_rows(tokens.astype(jnp.float32), gain_first).astype(jnp.bfloat16)
     hidden = folded(normed_first, first[0], first[1])
@@ -123,6 +125,7 @@
     base = base.astype(jnp.float32)
     extra = extra.astype(jnp.float32)
     middle = base + extra + 0.5 * first_sum
+    middle = lax.optimization_barrier(middle)
     normed_share = norm_rows(middle, gain_second).astype(jnp.bfloat16)
     coded = (normed_share.astype(jnp.float32) * A_SCALE).astype(jnp.float16)
     everyone = lax.all_gather(coded, TP, axis=0, tiled=True)

time: 184 us -> 182 us (0.989)
  no operation moved by 1% of the time
where the time goes in v3:
time: 182 us; the launch traced here: 181 us
  blocking collectives  135 us (74%)
  between operations  13.6 us (7%)
  starting transfers between devices  11.6 us (6%)
  matrix products  8.52 us (5%)
  other arithmetic  5.7 us (3%)
  waiting for transfers between devices  4.03 us (2%)
  local copies, waits for them, and re-layouts  2.92 us (2%)
    all_gather x1, blocking collectives, gather_weights(): first_z = lax.all_gather(first, 'z', axis=0, tiled=True)  37.7 us
    all_gather x1, blocking collectives, gather_weights(): lax.all_gather(first_z.reshape(NZ, rows, width), 'y', axis=1, tiled=True)  35.5 us
    all_to_all x2, blocking collectives, pieces_at_owner(): return lax.all_to_all(chip.reshape(NX, share, -1), 'x', 0, 0, tiled=True)  29.8 us
    all_gather x1, blocking collectives, body(): everyone = lax.all_gather(coded, TP, axis=0, tiled=True)  16.2 us
    all_gather x1, blocking collectives, spread_rows(): everyone = lax.all_gather(sent, TP, axis=0, tiled=True)  15.9 us
    ppermute x2, starting transfers between devices, swap_cores(): return lax.ppermute(x, 'c', [(0, 1), (1, 0)])  11.5 us
    ppermute x2, waiting for transfers between devices, swap_cores(): return lax.ppermute(x, 'c', [(0, 1), (1, 0)])  3.99 us
  transfers between devices with their start and end apart: 4, of which 2 were waited for; matrix products, arithmetic and copies ran while one was open for 3% of the time, Pallas kernels for 0%

profile of v3, /device:TPU:1, one launch (start us, length us, event | category | flops | bytes accessed | tf_op | source)
XLA Modules:
  0.0 181.3 jit_solution(12575469005783966153)
XLA Ops:
  6.5 0.0 copy-start
  6.5 0.0 all-gather.7.cloned.1.call-start
  6.5 1.6 fusion.36
  8.2 0.8 multiply_convert_fusion.23
  9.0 0.0 all-gather.7.cloned.1.call-update
  9.0 0.0 all-gather.9.cloned.1.call-start
  9.0 37.7 %all-gather.10 = f16[512,1152]{1,0:T(8,128)(2,1)S(1)} all-gather(f16[32,1152]{1,0:T(8,128)(2,1)S(1)} %multiply_convert_fusion.23), channel_id=1, replica_groups=mesh['z'=16,'y'=4,'x'=4,'c'=2] {'z'}, dimensions={0}, use_global_device_ids=true | all-gather | bytes 1253376 | tf_op jit(solution)/shard_map/all_gather | solution.py:42
  46.7 0.0 all-gather.7.cloned.1.call-done
  46.7 1.7 slice.36
  48.4 0.0 all-gather.9.cloned.1.call-update
  48.4 0.0 copy-done
  48.4 0.1 constant_dynamic-slice_fusion.5
  48.5 0.0 copy-start.1
  48.5 35.5 %all-gather.11 = f16[16,128,1152]{2,1,0:T(8,128)(2,1)S(1)} all-gather(f16[16,32,1152]{2,1,0:T(8,128)(2,1)S(1)} %bitcast.22), channel_id=1, replica_groups=mesh['z'=16,'y'=4,'x'=4,'c'=2] {'y'}, dimensions={1}, use_global_device_ids=true | all-gather | bytes 5898240 | tf_op jit(solution)/shard_map/all_gather | solution.py:47
  84.0 0.0 copy-done.1
  84.0 0.4 fusion
  84.4 0.3 copy-done.4
  84.7 1.0 fusion.3
  85.7 1.1 fusion.22
  86.8 0.1 constant_dynamic-slice_fusion.4
  86.9 0.7 convolution_convert_fusion.1
  87.7 9.5 %collective-permute-start = (bf16[192,2048]{1,0:T(8,128)(2,1)S(1)}, bf16[192,2048]{1,0:T(8,128)(2,1)S(1)}, u32[]{:S(2)}, u32[]{:S(2)}) collective-permute-start(bf16[192,2048]{1,0:T(8,128)(2,1)S(1)} %convolution_convert_fusion.1), channel_id=1, source_target_pairs={{0,1},{1,0},{2,3},{3,2},{4,5},{5,4},{6,7},{7,6},{8,9},{9,8},{10,11... | collective-permute-start | bytes 2359304 | tf_op jit(solution)/shard_map/ppermute | solution.py:22
  97.1 1.9 %collective-permute-done = bf16[192,2048]{1,0:T(8,128)(2,1)S(1)} collective-permute-done((bf16[192,2048]{1,0:T(8,128)(2,1)S(1)}, bf16[192,2048]{1,0:T(8,128)(2,1)S(1)}, u32[]{:S(2)}, u32[]{:S(2)}) %collective-permute-start) | collective-permute-done | bytes 786464 | tf_op jit(solution)/shard_map/ppermute | solution.py:22
  99.0 0.8 add_convert_fusion.1
  99.8 15.3 %all_to_all.10 = bf16[4,48,2048]{2,1,0:T(8,128)(2,1)S(1)} all-to-all(bf16[4,48,2048]{2,1,0:T(8,128)(2,1)S(1)} %bitcast.25), channel_id=1, replica_groups=mesh['z'=16,'y'=4,'x'=4,'c'=2] {'x'}, dimensions={0} | all-to-all | bytes 1572864 | tf_op jit(solution)/shard_map/all_to_all | solution.py:73
  115.1 0.1 convert_reduce_fusion.1
  115.2 0.1 multiply_add_fusion
  115.3 0.1 multiply_reduce_fusion
  115.4 0.3 copy-done.3
  115.8 0.1 multiply_convert_fusion.21
  115.9 16.2 %all-gather.12 = f16[384,2048]{1,0:T(8,128)(2,1)S(1)} all-gather(f16[48,2048]{1,0:T(8,128)(2,1)S(1)} %multiply_convert_fusion.21), channel_id=1, replica_groups=mesh['z'=16,'y'=4,'x'=4,'c'=2] {'x','c'}, dimensions={0}, use_global_device_ids=true | all-gather | bytes 1769472 | tf_op jit(solution)/shard_map/all_gather | solution.py:131
  132.1 2.5 %fusion.7 = f32[384,384]{1,0:T(8,128)S(1)} fusion(bf16[2048,1152]{1,0:T(8,128)(2,1)} %all-gather.9.cloned.1.call-done, f16[384,2048]{1,0:T(8,128)(2,1)S(1)} %all-gather.12), kind=kOutput, calls=%fused_computation.16 | convolution fusion | flops 606339072 | bytes 3735552 | tf_op jit(solution)/shard_map/dot_general | solution.py:57
  134.6 0.3 copy-done.2
  134.9 1.0 fusion.23
  135.9 0.7 convolution_convert_fusion
  136.7 2.1 %collective-permute-start.1 = (bf16[192,2048]{1,0:T(8,128)(2,1)S(1)}, bf16[192,2048]{1,0:T(8,128)(2,1)S(1)}, u32[]{:S(2)}, u32[]{:S(2)}) collective-permute-start(bf16[192,2048]{1,0:T(8,128)(2,1)S(1)} %convolution_convert_fusion), channel_id=1, source_target_pairs={{0,1},{1,0},{2,3},{3,2},{4,5},{5,4},{6,7},{7,6},{8,9},{9,8},{10,11... | collective-permute-start | bytes 2359304 | tf_op jit(solution)/shard_map/ppermute | solution.py:22
  138.7 2.1 %collective-permute-done.1 = bf16[192,2048]{1,0:T(8,128)(2,1)S(1)} collective-permute-done((bf16[192,2048]{1,0:T(8,128)(2,1)S(1)}, bf16[192,2048]{1,0:T(8,128)(2,1)S(1)}, u32[]{:S(2)}, u32[]{:S(2)}) %collective-permute-start.1) | collective-permute-done | bytes 786464 | tf_op jit(solution)/shard_map/ppermute | solution.py:22
  140.8 0.7 add_convert_fusion
  141.5 14.5 %all_to_all.11 = bf16[4,48,2048]{2,1,0:T(8,128)(2,1)S(1)} all-to-all(bf16[4,48,2048]{2,1,0:T(8,128)(2,1)S(1)} %bitcast.23), channel_id=1, replica_groups=mesh['z'=16,'y'=4,'x'=4,'c'=2] {'x'}, dimensions={0} | all-to-all | bytes 1572864 | tf_op jit(solution)/shard_map/all_to_all | solution.py:73
  156.1 0.1 convert_reduce_fusion
  156.2 0.2 fusion.33
  156.4 0.1 fusion.34
  156.5 0.1 broadcast_in_dim.119
  156.6 0.1 pad_maximum_fusion
  156.6 15.9 %all-gather.13 = f16[384,2176]{1,0:T(8,128)(2,1)S(1)} all-gather(f16[48,2176]{1,0:T(8,128)(2,1)S(1)} %pad_maximum_fusion), channel_id=1, replica_groups=mesh['z'=16,'y'=4,'x'=4,'c'=2] {'x','c'}, dimensions={0}, use_global_device_ids=true | all-gather | bytes 1880064 | tf_op jit(solution)/shard_map/all_gather | solution.py:98
  172.5 0.3 multiply_select_fusion
  172.9 0.1 reduce
  173.0 1.5 multiply_convert_fusion
  (9 shorter events, 0.1 us)
Async XLA Ops:
  6.5 41.9 %copy-start = (bf16[384,2048]{1,0:T(8,128)(2,1)S(1)}, bf16[384,2048]{1,0:T(8,128)(2,1)}, u32[]{:S(2)}) copy-start(bf16[384,2048]{1,0:T(8,128)(2,1)} %param.11) | copy-start | bytes 4718596
  6.5 40.2 %all-gather.7.cloned.1.call-start = ((), (), s32[]{:S(2)}) async-start(), calls=%async_computation.2 | async-start | bytes 1474560 | tf_op jit(solution)/shard_map/all_gather | solution.py:41
  9.0 123.1 %all-gather.9.cloned.1.call-start = ((), (), s32[]{:S(2)}) async-start(), calls=%async_computation.3 | async-start | bytes 5013504 | tf_op jit(solution)/shard_map/all_gather | solution.py:46
  48.5 35.5 %copy-start.1 = (bf16[384,2048]{1,0:T(8,128)(2,1)S(1)}, bf16[384,2048]{1,0:T(8,128)(2,1)}, u32[]{:S(2)}) copy-start(bf16[384,2048]{1,0:T(8,128)(2,1)} %param.10) | copy-start | bytes 4718596
  84.0 0.7 copy-start.4
  87.7 11.4 %collective-permute-start = (bf16[192,2048]{1,0:T(8,128)(2,1)S(1)}, bf16[192,2048]{1,0:T(8,128)(2,1)S(1)}, u32[]{:S(2)}, u32[]{:S(2)}) collective-permute-start(bf16[192,2048]{1,0:T(8,128)(2,1)S(1)} %convolution_convert_fusion.1), channel_id=1, source_target_pairs={{0,1},{1,0},{2,3},{3,2},{4,5},{5,4},{6,7},{7,6},{8,9},{9,8},{10,11... | collective-permute-start | bytes 2359304 | tf_op jit(solution)/shard_map/ppermute | solution.py:22
  115.1 0.7 copy-start.3
  132.1 2.8 %copy-start.2 = (bf16[2048,1152]{1,0:T(8,128)(2,1)S(1)}, bf16[2048,1152]{1,0:T(8,128)(2,1)}, u32[]{:S(2)}) copy-start(bf16[2048,1152]{1,0:T(8,128)(2,1)} %all-gather.9.cloned.1.call-done) | copy-start | bytes 14155780
  136.7 4.2 %collective-permute-start.1 = (bf16[192,2048]{1,0:T(8,128)(2,1)S(1)}, bf16[192,2048]{1,0:T(8,128)(2,1)S(1)}, u32[]{:S(2)}, u32[]{:S(2)}) collective-permute-start(bf16[192,2048]{1,0:T(8,128)(2,1)S(1)} %convolution_convert_fusion), channel_id=1, source_target_pairs={{0,1},{1,0},{2,3},{3,2},{4,5},{5,4},{6,7},{7,6},{8,9},{9,8},{10,11... | collective-permute-start | bytes 2359304 | tf_op jit(solution)/shard_map/ppermute | solution.py:22
Sparse Core Ops, SparseCore 0:
  9.4 35.3 all-gather.6
  48.5 72.4 all-gather.8

commit v4 on v0

--- a/solution.py
+++ b/solution.py
@@ -59,6 +59,12 @@
     return (jax.nn.silu(gate) * up).astype(jnp.bfloat16)
 
 
+def folded_at_once(normed, both_w):
+    both = jnp.dot(normed, both_w, preferred_element_type=jnp.float32)
+    half = both.shape[1] // 2
+    return (jax.nn.silu(both[:, :half]) * both[:, half:]).astype(jnp.bfloat16)
+
+
 def down_dot(hidden, down_t):
     return lax.dot_general(hidden, down_t, (((1,), (1,)), ((), ())), preferred_element_type=jnp.float32)
 
@@ -109,7 +115,8 @@
     offset, tokens = lax.optimization_barrier((offset, tokens))
     own_first = half_coded(side_by_side((gate_first, up_first, down_first.T)))
     own_second = side_by_side((gate_second, up_second, down_second.T), NY)
-    first, second = (thirds(whole) for whole in gather_weights(own_first, own_second))
+    first, second_whole = gather_weights(own_first, own_second)
+    first, second = thirds(first), thirds(second_whole)
     first = [plain(w) for w in first]
     normed_first = norm_rows(tokens.astype(jnp.float32), gain_first).astype(jnp.bfloat16)
     hidden = folded(normed_first, first[0], first[1])
@@ -123,7 +130,7 @@
     coded = (normed_share.astype(jnp.float32) * A_SCALE).astype(jnp.float16)
     everyone = lax.all_gather(coded, TP, axis=0, tiled=True)
     normed_second = (everyone.astype(jnp.float32) * (1.0 / A_SCALE)).astype(jnp.bfloat16)
-    hidden_two = folded(normed_second, second[0], second[1])
+    hidden_two = folded_at_once(normed_second, second_whole[:, : 2 * second[0].shape[1]])
     second_sum = added(pieces_at_owner(hidden_two, second[2], share))
     finished = (middle + 0.5 * second_sum).astype(jnp.bfloat16)
     return spread_rows(finished)

time: 182 us -> 182 us (level)
    dot_general x0 -> x1, matrix products: none -> 3.41 us  [folded_at_once(): both = jnp.dot(normed, both_w, preferred_element_type=jnp.float32)]
    dot_general x2 -> x1, matrix products: 3.56 us -> 1.03 us  [folded(): gate = jnp.dot(normed, gate_w, preferred_element_type=jnp.float32)]
where the time goes in v4:
time: 182 us; the launch traced here: 181 us
  blocking collectives  135 us (74%)
  between operations  13.6 us (7%)
  starting transfers between devices  11.5 us (6%)
  matrix products  8.42 us (5%)
  other arithmetic  6.88 us (4%)
  waiting for transfers between devices  4.03 us (2%)
  local copies, waits for them, and re-layouts  1.87 us (1%)
    all_gather x1, blocking collectives, gather_weights(): first_z = lax.all_gather(first, 'z', axis=0, tiled=True)  37.7 us
    all_gather x1, blocking collectives, gather_weights(): lax.all_gather(first_z.reshape(NZ, rows, width), 'y', axis=1, tiled=True)  35.5 us
    all_to_all x2, blocking collectives, pieces_at_owner(): return lax.all_to_all(chip.reshape(NX, share, -1), 'x', 0, 0, tiled=True)  29.8 us
    all_gather x1, blocking collectives, body(): everyone = lax.all_gather(coded, TP, axis=0, tiled=True)  16.3 us
    all_gather x1, blocking collectives, spread_rows(): everyone = lax.all_gather(sent, TP, axis=0, tiled=True)  15.9 us
    ppermute x2, starting transfers between devices, swap_cores(): return lax.ppermute(x, 'c', [(0, 1), (1, 0)])  11.5 us
    ppermute x2, waiting for transfers between devices, swap_cores(): return lax.ppermute(x, 'c', [(0, 1), (1, 0)])  3.99 us
  transfers between devices with their start and end apart: 4, of which 2 were waited for; matrix products, arithmetic and copies ran while one was open for 3% of the time, Pallas kernels for 0%

profile of v4, /device:TPU:1, one launch (start us, length us, event | category | flops | bytes accessed | tf_op | source)
XLA Modules:
  0.0 181.4 jit_solution(14467079372760481002)
XLA Ops:
  6.5 0.0 copy-start
  6.5 0.0 all-gather.7.cloned.1.call-start
  6.5 1.6 fusion.30
  8.2 0.8 multiply_convert_fusion.18
  9.0 0.0 all-gather.7.cloned.1.call-update
  9.0 0.0 all-gather.9.cloned.1.call-start
  9.0 37.7 %all-gather.10 = f16[512,1152]{1,0:T(8,128)(2,1)S(1)} all-gather(f16[32,1152]{1,0:T(8,128)(2,1)S(1)} %multiply_convert_fusion.18), channel_id=1, replica_groups=mesh['z'=16,'y'=4,'x'=4,'c'=2] {'z'}, dimensions={0}, use_global_device_ids=true | all-gather | bytes 1253376 | tf_op jit(solution)/shard_map/all_gather | solution.py:42
  46.7 0.0 all-gather.7.cloned.1.call-done
  46.7 1.7 slice.40
  48.4 0.0 all-gather.9.cloned.1.call-update
  48.4 0.0 copy-done
  48.4 0.4 fusion
  48.8 0.0 copy-start.3
  48.8 35.5 %all-gather.11 = f16[16,128,1152]{2,1,0:T(8,128)(2,1)S(1)} all-gather(f16[16,32,1152]{2,1,0:T(8,128)(2,1)S(1)} %bitcast.22), channel_id=1, replica_groups=mesh['z'=16,'y'=4,'x'=4,'c'=2] {'y'}, dimensions={1}, use_global_device_ids=true | all-gather | bytes 5898240 | tf_op jit(solution)/shard_map/all_gather | solution.py:47
  84.3 0.0 copy-done.3
  84.3 1.0 fusion.5
  85.4 1.1 fusion.18
  86.5 0.7 convolution_convert_fusion.1
  87.2 9.4 %collective-permute-start = (bf16[192,2048]{1,0:T(8,128)(2,1)S(1)}, bf16[192,2048]{1,0:T(8,128)(2,1)S(1)}, u32[]{:S(2)}, u32[]{:S(2)}) collective-permute-start(bf16[192,2048]{1,0:T(8,128)(2,1)S(1)} %convolution_convert_fusion.1), channel_id=1, source_target_pairs={{0,1},{1,0},{2,3},{3,2},{4,5},{5,4},{6,7},{7,6},{8,9},{9,8},{10,11... | collective-permute-start | bytes 2359304 | tf_op jit(solution)/shard_map/ppermute | solution.py:22
  96.7 1.9 %collective-permute-done = bf16[192,2048]{1,0:T(8,128)(2,1)S(1)} collective-permute-done((bf16[192,2048]{1,0:T(8,128)(2,1)S(1)}, bf16[192,2048]{1,0:T(8,128)(2,1)S(1)}, u32[]{:S(2)}, u32[]{:S(2)}) %collective-permute-start) | collective-permute-done | bytes 786464 | tf_op jit(solution)/shard_map/ppermute | solution.py:22
  98.6 0.8 add_convert_fusion.1
  99.3 15.3 %all_to_all.10 = bf16[4,48,2048]{2,1,0:T(8,128)(2,1)S(1)} all-to-all(bf16[4,48,2048]{2,1,0:T(8,128)(2,1)S(1)} %bitcast.26), channel_id=1, replica_groups=mesh['z'=16,'y'=4,'x'=4,'c'=2] {'x'}, dimensions={0} | all-to-all | bytes 1572864 | tf_op jit(solution)/shard_map/all_to_all | solution.py:79
  114.6 0.0 copy-start.2
  114.6 0.1 convert_reduce_fusion.1
  114.7 1.2 multiply_reduce_fusion
  115.9 0.0 copy-done.2
  116.0 0.1 multiply_convert_fusion.16
  116.1 16.3 %all-gather.12 = f16[384,2048]{1,0:T(8,128)(2,1)S(1)} all-gather(f16[48,2048]{1,0:T(8,128)(2,1)S(1)} %multiply_convert_fusion.16), channel_id=1, replica_groups=mesh['z'=16,'y'=4,'x'=4,'c'=2] {'x','c'}, dimensions={0}, use_global_device_ids=true | all-gather | bytes 1769472 | tf_op jit(solution)/shard_map/all_gather | solution.py:131
  132.4 0.0 all-gather.9.cloned.1.call-done
  132.4 0.0 copy-start.1
  132.4 3.4 %fusion.3 = f32[384,768]{1,0:T(8,128)S(1)} fusion(bf16[2048,1152]{1,0:T(8,128)(2,1)} %all-gather.9.cloned.1.call-done, f16[384,2048]{1,0:T(8,128)(2,1)S(1)} %all-gather.12), kind=kOutput, calls=%fused_computation.5 | convolution fusion | flops 1210318848 | bytes 5898240 | tf_op jit(solution)/shard_map/dot_general | solution.py:63
  135.8 0.2 fusion.20
  136.0 0.0 copy-done.1
  136.0 0.7 convolution_convert_fusion
  136.7 2.1 %collective-permute-start.1 = (bf16[192,2048]{1,0:T(8,128)(2,1)S(1)}, bf16[192,2048]{1,0:T(8,128)(2,1)S(1)}, u32[]{:S(2)}, u32[]{:S(2)}) collective-permute-start(bf16[192,2048]{1,0:T(8,128)(2,1)S(1)} %convolution_convert_fusion), channel_id=1, source_target_pairs={{0,1},{1,0},{2,3},{3,2},{4,5},{5,4},{6,7},{7,6},{8,9},{9,8},{10,11... | collective-permute-start | bytes 2359304 | tf_op jit(solution)/shard_map/ppermute | solution.py:22
  138.8 2.1 %collective-permute-done.1 = bf16[192,2048]{1,0:T(8,128)(2,1)S(1)} collective-permute-done((bf16[192,2048]{1,0:T(8,128)(2,1)S(1)}, bf16[192,2048]{1,0:T(8,128)(2,1)S(1)}, u32[]{:S(2)}, u32[]{:S(2)}) %collective-permute-start.1) | collective-permute-done | bytes 786464 | tf_op jit(solution)/shard_map/ppermute | solution.py:22
  140.9 0.7 add_convert_fusion
  141.6 14.5 %all_to_all.11 = bf16[4,48,2048]{2,1,0:T(8,128)(2,1)S(1)} all-to-all(bf16[4,48,2048]{2,1,0:T(8,128)(2,1)S(1)} %bitcast.23), channel_id=1, replica_groups=mesh['z'=16,'y'=4,'x'=4,'c'=2] {'x'}, dimensions={0} | all-to-all | bytes 1572864 | tf_op jit(solution)/shard_map/all_to_all | solution.py:79
  156.1 0.1 convert_reduce_fusion
  156.3 0.2 fusion.27
  156.5 0.1 fusion.28
  156.6 0.1 broadcast_in_dim.119
  156.7 0.1 pad_maximum_fusion
  156.7 15.9 %all-gather.13 = f16[384,2176]{1,0:T(8,128)(2,1)S(1)} all-gather(f16[48,2176]{1,0:T(8,128)(2,1)S(1)} %pad_maximum_fusion), channel_id=1, replica_groups=mesh['z'=16,'y'=4,'x'=4,'c'=2] {'x','c'}, dimensions={0}, use_global_device_ids=true | all-gather | bytes 1880064 | tf_op jit(solution)/shard_map/all_gather | solution.py:104
  172.6 0.3 multiply_select_fusion
  172.9 0.1 reduce
  173.1 1.5 multiply_convert_fusion
  (5 shorter events, 0.1 us)
Async XLA Ops:
  6.5 41.9 %copy-start = (bf16[384,2048]{1,0:T(8,128)(2,1)S(1)}, bf16[384,2048]{1,0:T(8,128)(2,1)}, u32[]{:S(2)}) copy-start(bf16[384,2048]{1,0:T(8,128)(2,1)} %param.10) | copy-start | bytes 4718596
  6.5 40.2 %all-gather.7.cloned.1.call-start = ((), (), s32[]{:S(2)}) async-start(), calls=%async_computation.2 | async-start | bytes 1474560 | tf_op jit(solution)/shard_map/all_gather | solution.py:41
  9.0 123.4 %all-gather.9.cloned.1.call-start = ((), (), s32[]{:S(2)}) async-start(), calls=%async_computation.3 | async-start | bytes 5013504 | tf_op jit(solution)/shard_map/all_gather | solution.py:46
  48.8 35.5 %copy-start.3 = (f32[2048]{0:T(1024)S(1)}, f32[2048]{0:T(1024)}, u32[]{:S(2)}) copy-start(f32[2048]{0:T(1024)} %param.12) | copy-start | bytes 24580
  87.2 11.3 %collective-permute-start = (bf16[192,2048]{1,0:T(8,128)(2,1)S(1)}, bf16[192,2048]{1,0:T(8,128)(2,1)S(1)}, u32[]{:S(2)}, u32[]{:S(2)}) collective-permute-start(bf16[192,2048]{1,0:T(8,128)(2,1)S(1)} %convolution_convert_fusion.1), channel_id=1, source_target_pairs={{0,1},{1,0},{2,3},{3,2},{4,5},{5,4},{6,7},{7,6},{8,9},{9,8},{10,11... | collective-permute-start | bytes 2359304 | tf_op jit(solution)/shard_map/ppermute | solution.py:22
  114.6 1.3 copy-start.2
  132.4 3.7 %copy-start.1 = (bf16[2048,1152]{1,0:T(8,128)(2,1)S(1)}, bf16[2048,1152]{1,0:T(8,128)(2,1)}, u32[]{:S(2)}) copy-start(bf16[2048,1152]{1,0:T(8,128)(2,1)} %all-gather.9.cloned.1.call-done) | copy-start | bytes 14155780
  136.7 4.2 %collective-permute-start.1 = (bf16[192,2048]{1,0:T(8,128)(2,1)S(1)}, bf16[192,2048]{1,0:T(8,128)(2,1)S(1)}, u32[]{:S(2)}, u32[]{:S(2)}) collective-permute-start(bf16[192,2048]{1,0:T(8,128)(2,1)S(1)} %convolution_convert_fusion), channel_id=1, source_target_pairs={{0,1},{1,0},{2,3},{3,2},{4,5},{5,4},{6,7},{7,6},{8,9},{9,8},{10,11... | collective-permute-start | bytes 2359304 | tf_op jit(solution)/shard_map/ppermute | solution.py:22
Sparse Core Ops, SparseCore 0:
  9.4 35.3 all-gather.6
  48.5 72.4 all-gather.8

commit v5 on v4

--- a/solution.py
+++ b/solution.py
@@ -51,12 +51,6 @@
 def thirds(whole):
     width = whole.shape[1] // 3
     return [whole[:, k * width : (k + 1) * width] for k in range(3)]
-
-
-def folded(normed, gate_w, up_w):
-    gate = jnp.dot(normed, gate_w, preferred_element_type=jnp.float32)
-    up = jnp.dot(normed, up_w, preferred_element_type=jnp.float32)
-    return (jax.nn.silu(gate) * up).astype(jnp.bfloat16)
 
 
 def folded_at_once(normed, both_w):
@@ -116,11 +110,12 @@
     own_first = half_coded(side_by_side((gate_first, up_first, down_first.T)))
     own_second = side_by_side((gate_second, up_second, down_second.T), NY)
     first, second_whole = gather_weights(own_first, own_second)
-    first, second = thirds(first), thirds(second_whole)
-    first = [plain(w) for w in first]
+    first_both = plain(first[:, : 2 * first.shape[1] // 3])
+    first_down = plain(thirds(first)[2])
+    second = thirds(second_whole)
     normed_first = norm_rows(tokens.astype(jnp.float32), gain_first).astype(jnp.bfloat16)
-    hidden = folded(normed_first, first[0], first[1])
-    pieces = pieces_at_owner(hidden, first[2], share)
+    hidden = folded_at_once(normed_first, first_both)
+    pieces = pieces_at_owner(hidden, first_down, share)
     pieces, tokens, merged, gain_second, offset = lax.optimization_barrier((pieces, tokens, merged, gain_second, offset))
     first_sum = added(pieces)
     base = lax.dynamic_slice_in_dim(tokens, offset, share, 0).astype(jnp.float32)

time: 182 us -> 182 us (level)
    dot_general x2 -> x0, matrix products: 2.1 us -> none  [the longest x1 1.07 us: folded(): up = jnp.dot(normed, up_w, preferred_element_type=jnp.float32)]
    dot_general x1 -> x2, matrix products: 3.41 us -> 4.98 us  [folded_at_once(): both = jnp.dot(normed, both_w, preferred_element_type=jnp.float32)]
where the time goes in v5:
time: 182 us; the launch traced here: 181 us
  blocking collectives  135 us (74%)
  between operations  13.6 us (7%)
  starting transfers between devices  11.5 us (6%)
  matrix products  7.91 us (4%)
  other arithmetic  7.05 us (4%)
  waiting for transfers between devices  4.03 us (2%)
  local copies, waits for them, and re-layouts  1.87 us (1%)
    all_gather x1, blocking collectives, gather_weights(): first_z = lax.all_gather(first, 'z', axis=0, tiled=True)  37.7 us
    all_gather x1, blocking collectives, gather_weights(): lax.all_gather(first_z.reshape(NZ, rows, width), 'y', axis=1, tiled=True)  35.5 us
    all_to_all x2, blocking collectives, pieces_at_owner(): return lax.all_to_all(chip.reshape(NX, share, -1), 'x', 0, 0, tiled=True)  29.8 us
    all_gather x1, blocking collectives, body(): everyone = lax.all_gather(coded, TP, axis=0, tiled=True)  16.3 us
    all_gather x1, blocking collectives, spread_rows(): everyone = lax.all_gather(sent, TP, axis=0, tiled=True)  15.9 us
    ppermute x2, starting transfers between devices, swap_cores(): return lax.ppermute(x, 'c', [(0, 1), (1, 0)])  11.5 us
    dot_general x2, matrix products, folded_at_once(): both = jnp.dot(normed, both_w, preferred_element_type=jnp.float32)  4.98 us
    ppermute x2, waiting for transfers between devices, swap_cores(): return lax.ppermute(x, 'c', [(0, 1), (1, 0)])  4 us
  transfers between devices with their start and end apart: 4, of which 2 were waited for; matrix products, arithmetic and copies ran while one was open for 3% of the time, Pallas kernels for 0%

profile of v5, /device:TPU:1, one launch (start us, length us, event | category | flops | bytes accessed | tf_op | source)
XLA Modules:
  0.0 181.2 jit_solution(18376802903462797789)
XLA Ops:
  6.5 0.0 copy-start
  6.5 0.0 all-gather.7.cloned.1.call-start
  6.5 1.6 fusion.27
  8.2 0.8 multiply_convert_fusion.12
  9.0 0.0 all-gather.7.cloned.1.call-update
  9.0 0.0 all-gather.9.cloned.1.call-start
  9.0 37.7 %all-gather.10 = f16[512,1152]{1,0:T(8,128)(2,1)S(1)} all-gather(f16[32,1152]{1,0:T(8,128)(2,1)S(1)} %multiply_convert_fusion.12), channel_id=1, replica_groups=mesh['z'=16,'y'=4,'x'=4,'c'=2] {'z'}, dimensions={0}, use_global_device_ids=true | all-gather | bytes 1253376 | tf_op jit(solution)/shard_map/all_gather | solution.py:42
  46.7 0.0 all-gather.7.cloned.1.call-done
  46.7 1.7 slice.44
  48.4 0.0 all-gather.9.cloned.1.call-update
  48.4 0.0 copy-done
  48.4 0.4 fusion
  48.8 0.0 copy-start.3
  48.8 35.5 %all-gather.11 = f16[16,128,1152]{2,1,0:T(8,128)(2,1)S(1)} all-gather(f16[16,32,1152]{2,1,0:T(8,128)(2,1)S(1)} %bitcast.21), channel_id=1, replica_groups=mesh['z'=16,'y'=4,'x'=4,'c'=2] {'y'}, dimensions={1}, use_global_device_ids=true | all-gather | bytes 5898240 | tf_op jit(solution)/shard_map/all_gather | solution.py:47
  84.3 0.0 copy-done.3
  84.3 1.6 fusion.3
  85.9 0.2 fusion.19
  86.1 0.7 convolution_convert_fusion.1
  86.9 9.4 %collective-permute-start = (bf16[192,2048]{1,0:T(8,128)(2,1)S(1)}, bf16[192,2048]{1,0:T(8,128)(2,1)S(1)}, u32[]{:S(2)}, u32[]{:S(2)}) collective-permute-start(bf16[192,2048]{1,0:T(8,128)(2,1)S(1)} %convolution_convert_fusion.1), channel_id=1, source_target_pairs={{0,1},{1,0},{2,3},{3,2},{4,5},{5,4},{6,7},{7,6},{8,9},{9,8},{10,11... | collective-permute-start | bytes 2359304 | tf_op jit(solution)/shard_map/ppermute | solution.py:22
  96.3 1.9 %collective-permute-done = bf16[192,2048]{1,0:T(8,128)(2,1)S(1)} collective-permute-done((bf16[192,2048]{1,0:T(8,128)(2,1)S(1)}, bf16[192,2048]{1,0:T(8,128)(2,1)S(1)}, u32[]{:S(2)}, u32[]{:S(2)}) %collective-permute-start) | collective-permute-done | bytes 786464 | tf_op jit(solution)/shard_map/ppermute | solution.py:22
  98.2 0.8 add_convert_fusion.1
  99.0 15.3 %all_to_all.10 = bf16[4,48,2048]{2,1,0:T(8,128)(2,1)S(1)} all-to-all(bf16[4,48,2048]{2,1,0:T(8,128)(2,1)S(1)} %bitcast.26), channel_id=1, replica_groups=mesh['z'=16,'y'=4,'x'=4,'c'=2] {'x'}, dimensions={0} | all-to-all | bytes 1572864 | tf_op jit(solution)/shard_map/all_to_all | solution.py:73
  114.3 0.0 copy-start.2
  114.3 0.1 convert_reduce_fusion.1
  114.4 1.2 multiply_reduce_fusion
  115.6 0.0 copy-done.2
  115.6 0.1 multiply_convert_fusion.10
  115.8 16.3 %all-gather.12 = f16[384,2048]{1,0:T(8,128)(2,1)S(1)} all-gather(f16[48,2048]{1,0:T(8,128)(2,1)S(1)} %multiply_convert_fusion.10), channel_id=1, replica_groups=mesh['z'=16,'y'=4,'x'=4,'c'=2] {'x','c'}, dimensions={0}, use_global_device_ids=true | all-gather | bytes 1769472 | tf_op jit(solution)/shard_map/all_gather | solution.py:126
  132.1 0.0 all-gather.9.cloned.1.call-done
  132.1 0.0 copy-start.1
  132.1 3.4 %fusion.4 = f32[384,768]{1,0:T(8,128)S(1)} fusion(bf16[2048,1152]{1,0:T(8,128)(2,1)} %all-gather.9.cloned.1.call-done, f16[384,2048]{1,0:T(8,128)(2,1)S(1)} %all-gather.12), kind=kOutput, calls=%fused_computation.7 | convolution fusion | flops 1210318848 | bytes 5898240 | tf_op jit(solution)/shard_map/dot_general | solution.py:57
  135.5 0.2 fusion.18
  135.7 0.0 copy-done.1
  135.7 0.7 convolution_convert_fusion
  136.5 2.1 %collective-permute-start.1 = (bf16[192,2048]{1,0:T(8,128)(2,1)S(1)}, bf16[192,2048]{1,0:T(8,128)(2,1)S(1)}, u32[]{:S(2)}, u32[]{:S(2)}) collective-permute-start(bf16[192,2048]{1,0:T(8,128)(2,1)S(1)} %convolution_convert_fusion), channel_id=1, source_target_pairs={{0,1},{1,0},{2,3},{3,2},{4,5},{5,4},{6,7},{7,6},{8,9},{9,8},{10,11... | collective-permute-start | bytes 2359304 | tf_op jit(solution)/shard_map/ppermute | solution.py:22
  138.5 2.1 %collective-permute-done.1 = bf16[192,2048]{1,0:T(8,128)(2,1)S(1)} collective-permute-done((bf16[192,2048]{1,0:T(8,128)(2,1)S(1)}, bf16[192,2048]{1,0:T(8,128)(2,1)S(1)}, u32[]{:S(2)}, u32[]{:S(2)}) %collective-permute-start.1) | collective-permute-done | bytes 786464 | tf_op jit(solution)/shard_map/ppermute | solution.py:22
  140.6 0.7 add_convert_fusion
  141.4 14.5 %all_to_all.11 = bf16[4,48,2048]{2,1,0:T(8,128)(2,1)S(1)} all-to-all(bf16[4,48,2048]{2,1,0:T(8,128)(2,1)S(1)} %bitcast.22), channel_id=1, replica_groups=mesh['z'=16,'y'=4,'x'=4,'c'=2] {'x'}, dimensions={0} | all-to-all | bytes 1572864 | tf_op jit(solution)/shard_map/all_to_all | solution.py:73
  155.9 0.1 convert_reduce_fusion
  156.0 0.2 fusion.24
  156.2 0.1 fusion.25
  156.3 0.1 broadcast_in_dim.119
  156.4 0.1 pad_maximum_fusion
  156.5 15.9 %all-gather.13 = f16[384,2176]{1,0:T(8,128)(2,1)S(1)} all-gather(f16[48,2176]{1,0:T(8,128)(2,1)S(1)} %pad_maximum_fusion), channel_id=1, replica_groups=mesh['z'=16,'y'=4,'x'=4,'c'=2] {'x','c'}, dimensions={0}, use_global_device_ids=true | all-gather | bytes 1880064 | tf_op jit(solution)/shard_map/all_gather | solution.py:98
  172.4 0.3 multiply_select_fusion
  172.7 0.1 reduce
  172.8 1.5 multiply_convert_fusion.2
  (5 shorter events, 0.1 us)
Async XLA Ops:
  6.5 41.9 %copy-start = (bf16[384,2048]{1,0:T(8,128)(2,1)S(1)}, bf16[384,2048]{1,0:T(8,128)(2,1)}, u32[]{:S(2)}) copy-start(bf16[384,2048]{1,0:T(8,128)(2,1)} %param.10) | copy-start | bytes 4718596
  6.5 40.2 %all-gather.7.cloned.1.call-start = ((), (), s32[]{:S(2)}) async-start(), calls=%async_computation.2 | async-start | bytes 1474560 | tf_op jit(solution)/shard_map/all_gather | solution.py:41
  9.0 123.1 %all-gather.9.cloned.1.call-start = ((), (), s32[]{:S(2)}) async-start(), calls=%async_computation.3 | async-start | bytes 5013504 | tf_op jit(solution)/shard_map/all_gather | solution.py:46
  48.8 35.5 %copy-start.3 = (f32[2048]{0:T(1024)S(1)}, f32[2048]{0:T(1024)}, u32[]{:S(2)}) copy-start(f32[2048]{0:T(1024)} %param.12) | copy-start | bytes 24580
  86.9 11.3 %collective-permute-start = (bf16[192,2048]{1,0:T(8,128)(2,1)S(1)}, bf16[192,2048]{1,0:T(8,128)(2,1)S(1)}, u32[]{:S(2)}, u32[]{:S(2)}) collective-permute-start(bf16[192,2048]{1,0:T(8,128)(2,1)S(1)} %convolution_convert_fusion.1), channel_id=1, source_target_pairs={{0,1},{1,0},{2,3},{3,2},{4,5},{5,4},{6,7},{7,6},{8,9},{9,8},{10,11... | collective-permute-start | bytes 2359304 | tf_op jit(solution)/shard_map/ppermute | solution.py:22
  114.3 1.3 copy-start.2
  132.1 3.7 %copy-start.1 = (bf16[2048,1152]{1,0:T(8,128)(2,1)S(1)}, bf16[2048,1152]{1,0:T(8,128)(2,1)}, u32[]{:S(2)}) copy-start(bf16[2048,1152]{1,0:T(8,128)(2,1)} %all-gather.9.cloned.1.call-done) | copy-start | bytes 14155780
  136.5 4.2 %collective-permute-start.1 = (bf16[192,2048]{1,0:T(8,128)(2,1)S(1)}, bf16[192,2048]{1,0:T(8,128)(2,1)S(1)}, u32[]{:S(2)}, u32[]{:S(2)}) collective-permute-start(bf16[192,2048]{1,0:T(8,128)(2,1)S(1)} %convolution_convert_fusion), channel_id=1, source_target_pairs={{0,1},{1,0},{2,3},{3,2},{4,5},{5,4},{6,7},{7,6},{8,9},{9,8},{10,11... | collective-permute-start | bytes 2359304 | tf_op jit(solution)/shard_map/ppermute | solution.py:22
Sparse Core Ops, SparseCore 0:
  9.4 35.3 all-gather.6
  48.5 72.3 all-gather.8

commit v6 on v3

--- a/solution.py
+++ b/solution.py
@@ -59,6 +59,12 @@
     return (jax.nn.silu(gate) * up).astype(jnp.bfloat16)
 
 
+def folded_at_once(normed, both_w):
+    both = jnp.dot(normed, both_w, preferred_element_type=jnp.float32)
+    half = both.shape[1] // 2
+    return (jax.nn.silu(both[:, :half]) * both[:, half:]).astype(jnp.bfloat16)
+
+
 def down_dot(hidden, down_t):
     return lax.dot_general(hidden, down_t, (((1,), (1,)), ((), ())), preferred_element_type=jnp.float32)
 
@@ -111,6 +117,7 @@
     own_second = side_by_side((gate_second, up_second, down_second.T), NY)
     first, second = gather_weights(own_first, own_second)
     first, tokens = lax.optimization_barrier((first, tokens))
+    second_whole = second
     first, second = thirds(first), thirds(second)
     first = [plain(w) for w in first]
     normed_first = norm_rows(tokens.astype(jnp.float32), gain_first).astype(jnp.bfloat16)
@@ -130,7 +137,7 @@
     coded = (normed_share.astype(jnp.float32) * A_SCALE).astype(jnp.float16)
     everyone = lax.all_gather(coded, TP, axis=0, tiled=True)
     normed_second = (everyone.astype(jnp.float32) * (1.0 / A_SCALE)).astype(jnp.bfloat16)
-    hidden_two = folded(normed_second, second[0], second[1])
+    hidden_two = folded_at_once(normed_second, second_whole[:, : 2 * second[0].shape[1]])
     second_sum = added(pieces_at_owner(hidden_two, second[2], share))
     finished = (middle + 0.5 * second_sum).astype(jnp.bfloat16)
     return spread_rows(finished)

time: 182 us -> 182 us (level)
    dot_general x0 -> x1, matrix products: none -> 3.41 us  [folded_at_once(): both = jnp.dot(normed, both_w, preferred_element_type=jnp.float32)]
    dot_general x2 -> x1, matrix products: 3.57 us -> 1.04 us  [folded(): gate = jnp.dot(normed, gate_w, preferred_element_type=jnp.float32)]
where the time goes in v6:
time: 182 us; the launch traced here: 181 us
  blocking collectives  135 us (74%)
  between operations  13.6 us (7%)
  starting transfers between devices  11.6 us (6%)
  matrix products  8.43 us (5%)
  other arithmetic  5.88 us (3%)
  waiting for transfers between devices  4.02 us (2%)
  local copies, waits for them, and re-layouts  2.63 us (1%)
    all_gather x1, blocking collectives, gather_weights(): first_z = lax.all_gather(first, 'z', axis=0, tiled=True)  37.7 us
    all_gather x1, blocking collectives, gather_weights(): lax.all_gather(first_z.reshape(NZ, rows, width), 'y', axis=1, tiled=True)  35.5 us
    all_to_all x2, blocking collectives, pieces_at_owner(): return lax.all_to_all(chip.reshape(NX, share, -1), 'x', 0, 0, tiled=True)  29.8 us
    all_gather x1, blocking collectives, body(): everyone = lax.all_gather(coded, TP, axis=0, tiled=True)  16.2 us
    all_gather x1, blocking collectives, spread_rows(): everyone = lax.all_gather(sent, TP, axis=0, tiled=True)  15.9 us
    ppermute x2, starting transfers between devices, swap_cores(): return lax.ppermute(x, 'c', [(0, 1), (1, 0)])  11.5 us
    ppermute x2, waiting for transfers between devices, swap_cores(): return lax.ppermute(x, 'c', [(0, 1), (1, 0)])  3.99 us
  transfers between devices with their start and end apart: 4, of which 2 were waited for; matrix products, arithmetic and copies ran while one was open for 3% of the time, Pallas kernels for 0%

profile of v6, /device:TPU:1, one launch (start us, length us, event | category | flops | bytes accessed | tf_op | source)
XLA Modules:
  0.0 181.1 jit_solution(9831467675801731277)
XLA Ops:
  6.5 0.0 copy-start
  6.5 0.0 all-gather.7.cloned.1.call-start
  6.5 1.6 fusion.30
  8.2 0.8 multiply_convert_fusion.18
  9.0 0.0 all-gather.7.cloned.1.call-update
  9.0 0.0 all-gather.9.cloned.1.call-start
  9.0 37.7 %all-gather.10 = f16[512,1152]{1,0:T(8,128)(2,1)S(1)} all-gather(f16[32,1152]{1,0:T(8,128)(2,1)S(1)} %multiply_convert_fusion.18), channel_id=1, replica_groups=mesh['z'=16,'y'=4,'x'=4,'c'=2] {'z'}, dimensions={0}, use_global_device_ids=true | all-gather | bytes 1253376 | tf_op jit(solution)/shard_map/all_gather | solution.py:42
  46.7 0.0 all-gather.7.cloned.1.call-done
  46.7 1.7 slice.40
  48.4 0.0 all-gather.9.cloned.1.call-update
  48.4 0.0 copy-done
  48.4 0.1 constant_dynamic-slice_fusion.5
  48.5 0.0 copy-start.1
  48.5 35.5 %all-gather.11 = f16[16,128,1152]{2,1,0:T(8,128)(2,1)S(1)} all-gather(f16[16,32,1152]{2,1,0:T(8,128)(2,1)S(1)} %bitcast.22), channel_id=1, replica_groups=mesh['z'=16,'y'=4,'x'=4,'c'=2] {'y'}, dimensions={1}, use_global_device_ids=true | all-gather | bytes 5898240 | tf_op jit(solution)/shard_map/all_gather | solution.py:47
  84.0 0.0 copy-done.1
  84.0 0.4 fusion
  84.4 0.3 copy-done.4
  84.7 1.0 fusion.5
  85.7 1.1 fusion.18
  86.8 0.1 constant_dynamic-slice_fusion.4
  86.9 0.7 convolution_convert_fusion.1
  87.7 9.5 %collective-permute-start = (bf16[192,2048]{1,0:T(8,128)(2,1)S(1)}, bf16[192,2048]{1,0:T(8,128)(2,1)S(1)}, u32[]{:S(2)}, u32[]{:S(2)}) collective-permute-start(bf16[192,2048]{1,0:T(8,128)(2,1)S(1)} %convolution_convert_fusion.1), channel_id=1, source_target_pairs={{0,1},{1,0},{2,3},{3,2},{4,5},{5,4},{6,7},{7,6},{8,9},{9,8},{10,11... | collective-permute-start | bytes 2359304 | tf_op jit(solution)/shard_map/ppermute | solution.py:22
  97.1 1.9 %collective-permute-done = bf16[192,2048]{1,0:T(8,128)(2,1)S(1)} collective-permute-done((bf16[192,2048]{1,0:T(8,128)(2,1)S(1)}, bf16[192,2048]{1,0:T(8,128)(2,1)S(1)}, u32[]{:S(2)}, u32[]{:S(2)}) %collective-permute-start) | collective-permute-done | bytes 786464 | tf_op jit(solution)/shard_map/ppermute | solution.py:22
  99.0 0.8 add_convert_fusion.1
  99.8 15.3 %all_to_all.10 = bf16[4,48,2048]{2,1,0:T(8,128)(2,1)S(1)} all-to-all(bf16[4,48,2048]{2,1,0:T(8,128)(2,1)S(1)} %bitcast.26), channel_id=1, replica_groups=mesh['z'=16,'y'=4,'x'=4,'c'=2] {'x'}, dimensions={0} | all-to-all | bytes 1572864 | tf_op jit(solution)/shard_map/all_to_all | solution.py:79
  115.1 0.1 convert_reduce_fusion.1
  115.2 0.1 multiply_add_fusion
  115.3 0.1 multiply_reduce_fusion
  115.4 0.3 copy-done.3
  115.8 0.1 multiply_convert_fusion.16
  115.9 16.2 %all-gather.12 = f16[384,2048]{1,0:T(8,128)(2,1)S(1)} all-gather(f16[48,2048]{1,0:T(8,128)(2,1)S(1)} %multiply_convert_fusion.16), channel_id=1, replica_groups=mesh['z'=16,'y'=4,'x'=4,'c'=2] {'x','c'}, dimensions={0}, use_global_device_ids=true | all-gather | bytes 1769472 | tf_op jit(solution)/shard_map/all_gather | solution.py:138
  132.1 3.4 %fusion.3 = f32[384,768]{1,0:T(8,128)S(1)} fusion(bf16[2048,1152]{1,0:T(8,128)(2,1)} %all-gather.9.cloned.1.call-done, f16[384,2048]{1,0:T(8,128)(2,1)S(1)} %all-gather.12), kind=kOutput, calls=%fused_computation.5 | convolution fusion | flops 1210318848 | bytes 5898240 | tf_op jit(solution)/shard_map/dot_general | solution.py:63
  135.5 0.2 fusion.20
  135.7 0.0 copy-done.2
  135.7 0.7 convolution_convert_fusion
  136.4 2.1 %collective-permute-start.1 = (bf16[192,2048]{1,0:T(8,128)(2,1)S(1)}, bf16[192,2048]{1,0:T(8,128)(2,1)S(1)}, u32[]{:S(2)}, u32[]{:S(2)}) collective-permute-start(bf16[192,2048]{1,0:T(8,128)(2,1)S(1)} %convolution_convert_fusion), channel_id=1, source_target_pairs={{0,1},{1,0},{2,3},{3,2},{4,5},{5,4},{6,7},{7,6},{8,9},{9,8},{10,11... | collective-permute-start | bytes 2359304 | tf_op jit(solution)/shard_map/ppermute | solution.py:22
  138.5 2.1 %collective-permute-done.1 = bf16[192,2048]{1,0:T(8,128)(2,1)S(1)} collective-permute-done((bf16[192,2048]{1,0:T(8,128)(2,1)S(1)}, bf16[192,2048]{1,0:T(8,128)(2,1)S(1)}, u32[]{:S(2)}, u32[]{:S(2)}) %collective-permute-start.1) | collective-permute-done | bytes 786464 | tf_op jit(solution)/shard_map/ppermute | solution.py:22
  140.6 0.7 add_convert_fusion
  141.3 14.5 %all_to_all.11 = bf16[4,48,2048]{2,1,0:T(8,128)(2,1)S(1)} all-to-all(bf16[4,48,2048]{2,1,0:T(8,128)(2,1)S(1)} %bitcast.23), channel_id=1, replica_groups=mesh['z'=16,'y'=4,'x'=4,'c'=2] {'x'}, dimensions={0} | all-to-all | bytes 1572864 | tf_op jit(solution)/shard_map/all_to_all | solution.py:79
  155.9 0.1 convert_reduce_fusion
  156.0 0.2 fusion.27
  156.2 0.1 fusion.28
  156.3 0.1 broadcast_in_dim.119
  156.4 0.1 pad_maximum_fusion
  156.4 15.9 %all-gather.13 = f16[384,2176]{1,0:T(8,128)(2,1)S(1)} all-gather(f16[48,2176]{1,0:T(8,128)(2,1)S(1)} %pad_maximum_fusion), channel_id=1, replica_groups=mesh['z'=16,'y'=4,'x'=4,'c'=2] {'x','c'}, dimensions={0}, use_global_device_ids=true | all-gather | bytes 1880064 | tf_op jit(solution)/shard_map/all_gather | solution.py:104
  172.3 0.3 multiply_select_fusion
  172.7 0.1 reduce
  172.8 1.5 multiply_convert_fusion
  (9 shorter events, 0.1 us)
Async XLA Ops:
  6.5 41.9 %copy-start = (bf16[384,2048]{1,0:T(8,128)(2,1)S(1)}, bf16[384,2048]{1,0:T(8,128)(2,1)}, u32[]{:S(2)}) copy-start(bf16[384,2048]{1,0:T(8,128)(2,1)} %param.11) | copy-start | bytes 4718596
  6.5 40.2 %all-gather.7.cloned.1.call-start = ((), (), s32[]{:S(2)}) async-start(), calls=%async_computation.2 | async-start | bytes 1474560 | tf_op jit(solution)/shard_map/all_gather | solution.py:41
  9.0 123.1 %all-gather.9.cloned.1.call-start = ((), (), s32[]{:S(2)}) async-start(), calls=%async_computation.3 | async-start | bytes 5013504 | tf_op jit(solution)/shard_map/all_gather | solution.py:46
  48.5 35.5 %copy-start.1 = (bf16[384,2048]{1,0:T(8,128)(2,1)S(1)}, bf16[384,2048]{1,0:T(8,128)(2,1)}, u32[]{:S(2)}) copy-start(bf16[384,2048]{1,0:T(8,128)(2,1)} %param.10) | copy-start | bytes 4718596
  84.0 0.7 copy-start.4
  87.7 11.4 %collective-permute-start = (bf16[192,2048]{1,0:T(8,128)(2,1)S(1)}, bf16[192,2048]{1,0:T(8,128)(2,1)S(1)}, u32[]{:S(2)}, u32[]{:S(2)}) collective-permute-start(bf16[192,2048]{1,0:T(8,128)(2,1)S(1)} %convolution_convert_fusion.1), channel_id=1, source_target_pairs={{0,1},{1,0},{2,3},{3,2},{4,5},{5,4},{6,7},{7,6},{8,9},{9,8},{10,11... | collective-permute-start | bytes 2359304 | tf_op jit(solution)/shard_map/ppermute | solution.py:22
  115.1 0.7 copy-start.3
  132.1 3.7 %copy-start.2 = (bf16[2048,1152]{1,0:T(8,128)(2,1)S(1)}, bf16[2048,1152]{1,0:T(8,128)(2,1)}, u32[]{:S(2)}) copy-start(bf16[2048,1152]{1,0:T(8,128)(2,1)} %all-gather.9.cloned.1.call-done) | copy-start | bytes 14155780
  136.4 4.2 %collective-permute-start.1 = (bf16[192,2048]{1,0:T(8,128)(2,1)S(1)}, bf16[192,2048]{1,0:T(8,128)(2,1)S(1)}, u32[]{:S(2)}, u32[]{:S(2)}) collective-permute-start(bf16[192,2048]{1,0:T(8,128)(2,1)S(1)} %convolution_convert_fusion), channel_id=1, source_target_pairs={{0,1},{1,0},{2,3},{3,2},{4,5},{5,4},{6,7},{7,6},{8,9},{9,8},{10,11... | collective-permute-start | bytes 2359304 | tf_op jit(solution)/shard_map/ppermute | solution.py:22
Sparse Core Ops, SparseCore 0:
  9.4 35.3 all-gather.6
  48.5 72.4 all-gather.8
